TPU v7x, 32 devices: a whole 2x2x4 slice. The times are simulated.
32 devices in a mesh: grp: 2 (over y), fs: 4 (over z), tp: 4 (over x, core).
Axes of the slice: x: 2, y: 2, z: 4, core: 2. Of those that a mesh axis runs over, the one named last changes fastest.
Arguments:
- tokens: bfloat16 [4096, 2048], P(('grp', 'fs', 'tp')), parts along dimension 0, may hold values from -6 to 6
- mix_weight_in: bfloat16 [2048, 1024], P('fs', 'tp'), may hold values from -0.125 to 0.125
- pool_scale: float32 [1024], P('tp'), may hold values from 0.1 to 1.9
- mix_weight_out: bfloat16 [1024, 2048], P('tp', 'fs'), may hold values from -0.1875 to 0.1875
- up_weight: bfloat16 [2048, 8192], P('fs', 'tp'), may hold values from -0.125 to 0.125
- down_weight: bfloat16 [8192, 2048], P('tp', 'fs'), may hold values from -0.0625 to 0.0625
- gains: float32 [4, 2048], replicated, may hold values from 0.1 to 1.9
Outputs:
- result: bfloat16 [4096, 2048], P(('grp', 'fs', 'tp')), parts along dimension 0
There are 2 independent parts, one for each index of `grp`. A program takes and returns all parts, laid end to end along the dimension named above; an argument that names none is the same for every part. Nothing has to cross between parts.
All inputs are finite; a program needn't handle non-finite values.
Results may differ from a plain program's by a relative error of at most 0.02.
Values may be sent and summed in bfloat16 or wider, within the bound.
A program may use at most 64 MiB of HBM per device.

v0:
```python
import functools

import jax
import jax.numpy as jnp
from jax import lax
from jax.experimental import pallas as pl
from jax.experimental.pallas import tpu as pltpu
from jax.sharding import PartitionSpec as P

GROUPS = 4
EPS = 1e-06
MESH = pl.DeviceIdType.MESH


def normalize(values, gain):
    upcast = values.astype(jnp.float32)
    return upcast * lax.rsqrt(jnp.mean(upcast * upcast, axis=-1, keepdims=True) + EPS) * gain


def pooling(mixed_in, first_channel, group_width):
    length, width = mixed_in.shape
    upcast = mixed_in.astype(jnp.float32)
    row = lax.broadcasted_iota(jnp.int32, (length, width), 0)
    group = (first_channel + lax.broadcasted_iota(jnp.int32, (length, width), 1)) // group_width
    position = (row + 1).astype(jnp.float32)
    total, average = upcast, jnp.zeros_like(upcast)
    for index in range(GROUPS):
        step = 1 << index
        total = total + jnp.where(row >= step, pltpu.roll(total, step, axis=0), 0.0)
        mean = total / jnp.minimum(position, float(2 * step))
        average = jnp.where(group == index, mean, average)
    return average - upcast


def kernel(dims, tok, gains, scale, mi_h, mo_h, up_h, dn_h, out,
           mi, mo, up, dn, g1, g2, hid, sp1, rq1, rp1, sp2, rq2, rp2, mid,
           lsem, zs_r, zs_l, zr, ys, yr, g1s, g1r, g2s, g2r, g3s, g3r, es, er,
           w1s, w1r, w2s, w2r, p1s, p1r, p2s, p2r, p3s):
    G, F, T, R, D, K, PWt, Ht, NU, ND = dims
    g, f, t = lax.axis_index("grp"), lax.axis_index("fs"), lax.axis_index("tp")
    cu, cd = Ht // NU, K // ND
    off = F >= 4
    far = F - 2 if off else F - 1
    first, last = (1, F - 2) if off else (0, F - 1)
    mid_plane = (f >= first) & (f <= last)
    end = (f < first) | (f > last)
    helper = (f == 1) | (f == F - 2) if off else f < 0
    helped = jnp.where(f == 1, 0, F - 1)
    inner = jnp.where(f == 0, 1, F - 2)
    sibling = t + 1 - 2 * lax.rem(t, 2)
    place, half_t = lax.rem(t, 2), T // 2
    step = D // 4

    def to_right_ok(w):
        return f + 1 < F if w in ("mi", "mo") else (f + 1 <= last)

    def to_left_ok(w):
        return f > 0 if w in ("mi", "mo") else (f - 1 >= first)

    def shared(w, s):
        return True if w in ("mi", "mo") or not off else ~(helper & (s == helped))
    pieces = {"mi": (0, 1), "mo": (1, 1), "up": (2, NU), "dn": (2 + NU, ND)}
    bufs = {"mi": (mi_h, mi), "mo": (mo_h, mo), "up": (up_h, up), "dn": (dn_h, dn)}

    def mult(value, by):
        return pl.multiple_of(value, by)

    def span(w, s, c, half):
        base = 0 if s is None else s * K
        if w == "mi":
            return pl.ds(mult(base + half * (K // G), K // G), K // G), pl.ds(0, PWt)
        if w == "mo":
            return pl.ds(mult(half * (PWt // G), PWt // G), PWt // G), pl.ds(mult(base, 128), K)
        if w == "up":
            return pl.ds(mult(base + half * (K // G), K // G), K // G), pl.ds(mult(c * cu, cu), cu)
        return pl.ds(mult(half * (Ht // G), Ht // G), Ht // G), pl.ds(mult(base + c * cd, cd), cd)

    def view(w, s, c, half):
        return bufs[w][1].at[span(w, s, c, half)]

    def z_copy(w, s, c, to_right, own=False):
        p = pieces[w][0] + c
        src = bufs[w][0].at[span(w, None, c, g)] if own else view(w, s, c, g)
        target = f + 1 if to_right else f - 1
        sems = zs_r if to_right else zs_l
        return pltpu.make_async_remote_copy(
            src_ref=src, dst_ref=view(w, s, c, g), send_sem=sems.at[s, p], recv_sem=zr.at[s, p],
            device_id=(g, target, t), device_id_type=MESH)

    def y_copy(w, s, c, k, half=None):
        p = pieces[w][0] + c
        half = g if half is None else half
        return pltpu.make_async_remote_copy(
            src_ref=view(w, s, c, half), dst_ref=view(w, s, c, half),
            send_sem=ys.at[k - 1, s, p], recv_sem=yr.at[k - 1, s, p],
            device_id=(lax.rem(g + k, G), f, t), device_id_type=MESH)

    def send_own(w, c):
        @pl.when(to_right_ok(w))
        def _():
            z_copy(w, f, c, True, own=True).start()

        @pl.when(to_left_ok(w))
        def _():
            z_copy(w, f, c, False, own=True).start()

    def whole_copy(w, c, k):
        p = pieces[w][0] + c
        half = lax.rem(g - k + G, G)
        return pltpu.make_async_remote_copy(
            src_ref=bufs[w][0].at[span(w, None, c, half)], dst_ref=view(w, f, c, half),
            send_sem=ys.at[k - 1, f, p], recv_sem=yr.at[k - 1, f, p],
            device_id=(g, inner, t), device_id_type=MESH)

    def send_whole(w):
        if off:
            @pl.when(end)
            def _():
                for c in range(pieces[w][1]):
                    for k in range(1, G):
                        whole_copy(w, c, k).start()

    def pump(w, d, c):
        for to_right in (True, False):
            s = f - d if to_right else f + d
            more = to_right_ok(w) if to_right else to_left_ok(w)
            here = (s >= 0) & (s < F)
            if w in ("up", "dn"):
                here = here & mid_plane

            @pl.when(here)
            def _():
                z_copy(w, s, c, to_right).wait_recv()

                @pl.when(more)
                def _():
                    z_copy(w, s, c, to_right).start()

                @pl.when(shared(w, s))
                def _():
                    for k in range(1, G):
                        y_copy(w, s, c, k).start()

    def y_wait(w, s, c):
        for k in range(1, G):
            y_copy(w, s, c, k, lax.rem(g - k + G, G)).wait_recv()

    def y_wait_all(w):
        def body(i, _):
            s, c = i // pieces[w][1], lax.rem(i, pieces[w][1])

            @pl.when(s != f)
            def _():
                y_wait(w, s, c)
            return 0
        lax.fori_loop(0, F * pieces[w][1], body, 0)

    def local(w, index):
        cols, rows = pl.ds(mult(f * K, K), K), pl.ds(mult(f * K, K), K)
        dst = bufs[w][1].at[rows, :] if w in ("mi", "up") else bufs[w][1].at[:, cols]
        return pltpu.make_async_copy(bufs[w][0], dst, lsem.at[index])

    def peer(k):
        return lax.rem(t + k, T)

    def tp_copy(src, dst, send, recv, k):
        return pltpu.make_async_remote_copy(
            src_ref=src, dst_ref=dst, send_sem=send, recv_sem=recv,
            device_id=(g, f, peer(k)), device_id_type=MESH)

    def gather_copy(buf, sems, block, target, row, index):
        return pltpu.make_async_remote_copy(
            src_ref=buf.at[block], dst_ref=buf.at[block], send_sem=sems[0].at[row, index],
            recv_sem=sems[1].at[block], device_id=(g, f, target), device_id_type=MESH)

    def gather_start(buf, sems):
        for k in range(2, T, 2):
            gather_copy(buf, sems, t, peer(k), 1, peer(k)).start()
        gather_copy(buf, sems, t, sibling, 0, t).start()

    def gather_finish(buf, sems):
        for k in range(2, T, 2):
            block = lax.rem(t - k + T, T)
            gather_copy(buf, sems, block, sibling, 0, block).wait_recv()
            gather_copy(buf, sems, block, sibling, 0, block).start()
        for k in range(0, T, 2):
            block = lax.rem(sibling - k + T, T)
            gather_copy(buf, sems, block, sibling, 0, block).wait_recv()

    def gather_drain(buf, sems):
        for k in range(2, T, 2):
            gather_copy(buf, sems, t, peer(k), 1, peer(k)).wait_send()
        for k in range(0, T, 2):
            block = lax.rem(t - k + T, T)
            gather_copy(buf, sems, block, sibling, 0, block).wait_send()

    own_rows, end_rows = g2.at[0], g2.at[1]
    sems1, sems2, sems3 = (g1s, g1r), (g2s, g2r), (g3s, g3r)

    def end_copy():
        return pltpu.make_async_remote_copy(
            src_ref=g2.at[0, t], dst_ref=g2.at[1, t], send_sem=es.at[0], recv_sem=er.at[0],
            device_id=(g, inner, t), device_id_type=MESH)

    def swap1(j):
        cols = pl.ds(j * step, step)
        return pltpu.make_async_remote_copy(
            src_ref=sp1.at[1 - place, :, :, cols], dst_ref=rq1.at[:, :, cols],
            send_sem=w1s.at[j], recv_sem=w1r.at[j], device_id=(g, f, sibling), device_id_type=MESH)

    def part1(k):
        return tp_copy(sp1.at[place, peer(k) // 2], rp1.at[k // 2 - 1],
                       p1s.at[k // 2 - 1], p1r.at[k // 2 - 1], k)

    def columns(s, c):
        return pl.ds(mult(s * K + c * cd, cd), cd)

    def swap2(i, s, c):
        return pltpu.make_async_remote_copy(
            src_ref=sp2.at[i, 1 - place, :, :, columns(s, c)], dst_ref=rq2.at[i, :, :, columns(s, c)],
            send_sem=w2s.at[i, s, c], recv_sem=w2r.at[i, s, c],
            device_id=(g, f, sibling), device_id_type=MESH)

    def part2(s, c, k):
        return tp_copy(sp2.at[0, place, peer(k) // 2, :, columns(s, c)], rp2.at[k // 2, :, columns(s, c)],
                       p2s.at[k // 2 - 1, s, c], p2r.at[k // 2, s, c], k)

    def part3(s, c, k):
        return pltpu.make_async_remote_copy(
            src_ref=sp2.at[1, place, peer(k) // 2, :, columns(s, c)], dst_ref=rp2.at[k // 2, :, columns(s, c)],
            send_sem=p3s.at[k // 2, s, c], recv_sem=p2r.at[k // 2, s, c],
            device_id=(g, helped, peer(k)), device_id_type=MESH)

    def merge(a, b):
        return (a.astype(jnp.float32) + b.astype(jnp.float32)).astype(jnp.bfloat16)

    barrier = pltpu.get_barrier_semaphore()

    @pl.when(f + 1 < F)
    def _():
        pl.semaphore_signal(barrier, inc=1, device_id=(g, f + 1, t), device_id_type=MESH)

    @pl.when(f > 0)
    def _():
        pl.semaphore_signal(barrier, inc=1, device_id=(g, f - 1, t), device_id_type=MESH)

    for k in range(1, G):
        pl.semaphore_signal(barrier, inc=1, device_id=(lax.rem(g + k, G), f, t), device_id_type=MESH)
    for k in range(1, T):
        pl.semaphore_signal(barrier, inc=1, device_id=(g, f, peer(k)), device_id_type=MESH)
    greeted = jnp.where(f + 1 < F, 1, 0) + jnp.where(f > 0, 1, 0) + (G - 1 + T - 1)
    if off:
        @pl.when(helper)
        def _():
            for k in range(1, T):
                pl.semaphore_signal(barrier, inc=1, device_id=(g, helped, peer(k)), device_id_type=MESH)

        @pl.when(end)
        def _():
            for k in range(1, T):
                pl.semaphore_signal(barrier, inc=1, device_id=(g, inner, peer(k)), device_id_type=MESH)
        greeted = greeted + jnp.where(helper | end, T - 1, 0)
    pl.semaphore_wait(barrier, greeted)

    send_own("mi", 0)
    send_own("mo", 0)
    send_own("up", 0)
    for index, w in enumerate(("mi", "mo", "up", "dn")):
        local(w, index).start()

    g1[t] = normalize(tok[...], gains[0:1, :]).astype(jnp.bfloat16)
    gather_start(g1, sems1)

    for d in range(1, F):
        pump("mi", d, 0)
        pump("mo", d, 0)
        if d < NU:
            send_own("up", d)
    for c in range(F, NU):
        send_own("up", c)
    send_whole("up")

    for c in range(NU // 2):
        pump("up", 1, c)

    y_wait_all("mi")
    local("mi", 0).wait()
    gather_finish(g1, sems1)
    mixed_in = jnp.dot(g1[...].reshape(T * R, D), mi[...],
                       preferred_element_type=jnp.float32).astype(jnp.bfloat16)
    scaled = (pooling(mixed_in, t * PWt, PWt * T // GROUPS) * scale[...]).astype(jnp.bfloat16)
    y_wait_all("mo")
    local("mo", 1).wait()
    for j in range(4):
        cols = pl.ds(j * step, step)
        value = jnp.dot(scaled, mo[:, cols], preferred_element_type=jnp.float32
                        ).astype(jnp.bfloat16).reshape(half_t, 2, R, step)
        for q in range(2):
            sp1[q, :, :, cols] = value[:, q]
        swap1(j).start()
    for j in range(4):
        cols = pl.ds(j * step, step)
        swap1(j).wait_recv()
        sp1[place, :, :, cols] = merge(sp1[place, :, :, cols], rq1[:, :, cols])
    for k in range(2, T, 2):
        part1(k).start()

    def pump_all(w, d, start=0):
        def body(c, _):
            pump(w, d, c)
            return 0
        lax.fori_loop(start, pieces[w][1], body, 0)

    pump_all("up", 1, NU // 2)
    early = far <= 2

    @pl.when(mid_plane & early)
    def _():
        for c in range(ND):
            send_own("dn", c)

    total = sp1[place, t // 2].astype(jnp.float32)
    for k in range(2, T, 2):
        part1(k).wait_recv()
        total = total + rp1[k // 2 - 1].astype(jnp.float32)
    mixer_out = total.astype(jnp.bfloat16)
    middle = (tok[...].astype(jnp.float32) + normalize(mixer_out, gains[1:2, :])).astype(jnp.bfloat16)
    mid[...] = middle
    g2[0, t] = normalize(middle, gains[2:3, :]).astype(jnp.bfloat16)

    @pl.when(mid_plane)
    def _():
        gather_start(own_rows, sems2)
    if off:
        @pl.when(end)
        def _():
            end_copy().start()

    def pump_mid(d, _):
        pump_all("up", d)
        return 0
    lax.fori_loop(2, far, pump_mid, 0)

    @pl.when(~(mid_plane & early))
    def _():
        for c in range(ND):
            send_own("dn", c)
    send_whole("dn")
    if far > 1:
        pump_all("up", far)

    width = 256

    def up_project(i):
        def up_step(j, _):
            cols = pl.ds(mult(j * width, width), width)
            pre = jnp.dot(g2[i].reshape(T * R, D), up[:, cols], preferred_element_type=jnp.float32)
            pre = jnp.maximum(pre, 0.0)
            hid[i, :, cols] = (pre * pre).astype(jnp.bfloat16)
            return 0
        lax.fori_loop(0, Ht // width, up_step, 0)

    local("up", 2).wait()
    local("dn", 3).wait()

    @pl.when(mid_plane)
    def _():
        gather_finish(own_rows, sems2)
        if off:
            @pl.when(helper)
            def _():
                end_copy().wait_recv()
                gather_start(end_rows, sems3)
        y_wait_all("up")
        up_project(0)
        for c in range(ND // 2):
            pump("dn", 1, c)
        if off:
            @pl.when(helper)
            def _():
                gather_finish(end_rows, sems3)
                up_project(1)

    def dn_compute(s, c):
        @pl.when(s != f)
        def _():
            y_wait("dn", s, c)
        cols = columns(s, c)

        def project(i):
            value = jnp.dot(hid[i], dn[:, cols], preferred_element_type=jnp.float32
                            ).astype(jnp.bfloat16).reshape(half_t, 2, R, cd)
            for q in range(2):
                sp2[i, q, :, :, cols] = value[:, q]
            swap2(i, s, c).start()
        if off:
            @pl.when(helper)
            def _():
                project(1)
        project(0)

    def dn_merge(s, c):
        cols = columns(s, c)

        def finish(i):
            swap2(i, s, c).wait_recv()
            sp2[i, place, :, :, cols] = merge(sp2[i, place, :, :, cols], rq2[i, :, :, cols])
        if off:
            @pl.when(helper)
            def _():
                finish(1)
                for k in range(0, T, 2):
                    part3(s, c, k).start()
        finish(0)
        for k in range(2, T, 2):
            part2(s, c, k).start()

    def dn_step(e, _):
        d, c = e // ND, lax.rem(e, ND)

        @pl.when((d <= far) & (e >= ND + ND // 2))
        def _():
            pump("dn", d, c)

        def one(j, _):
            now = j // 4
            late = lax.rem(j, 4) // 2
            side = lax.rem(j, 2)
            ev = e - 1 + now - ND + late * (ND - 1)
            dd, cc = ev // ND, lax.rem(ev, ND)
            s = f + (2 * side - 1) * dd
            right_turn = jnp.where(late == 1, dd == far, dd < far)
            once = (dd > 0) | (side == 0)
            wanted = (ev >= 0) & right_turn & once & (s >= 0) & (s < F)

            @pl.when(wanted & (now == 0))
            def _():
                dn_merge(s, cc)

            @pl.when(wanted & (now == 1))
            def _():
                dn_compute(s, cc)
            return 0
        lax.fori_loop(0, 8, one, 0)
        return 0

    @pl.when(mid_plane)
    def _():
        lax.fori_loop(ND, (far + 1) * ND + 2, dn_step, 0)

    def take(i, _):
        s, c = i // ND, lax.rem(i, ND)
        for k in range(2, T, 2):
            part2(s, c, k).wait_recv()
        if off:
            @pl.when(end)
            def _():
                part3(s, c, 0).wait_recv()
        return 0
    lax.fori_loop(0, F * ND, take, 0)

    @pl.when(mid_plane)
    def _():
        rp2[0] = sp2[0, place, t // 2]
    total = jnp.zeros((R, D), jnp.float32)
    for k in range(half_t):
        total = total + rp2[k].astype(jnp.float32)
    channel_out = total.astype(jnp.bfloat16)
    out[...] = (mid[...].astype(jnp.float32) + normalize(channel_out, gains[3:4, :])).astype(jnp.bfloat16)

    for w in ("mi", "mo", "up", "dn"):
        def drain(i, _):
            s, c = i // pieces[w][1], lax.rem(i, pieces[w][1])

            moved = True if w in ("mi", "mo") else (mid_plane | (s == f))

            @pl.when((s <= f) & to_right_ok(w) & moved)
            def _():
                z_copy(w, s, c, True).wait_send()

            @pl.when((s >= f) & to_left_ok(w) & moved)
            def _():
                z_copy(w, s, c, False).wait_send()

            @pl.when((s != f) & moved & shared(w, s))
            def _():
                for k in range(1, G):
                    y_copy(w, s, c, k).wait_send()
            if off and w in ("up", "dn"):
                @pl.when((s == f) & end)
                def _():
                    for k in range(1, G):
                        whole_copy(w, c, k).wait_send()
            return 0
        lax.fori_loop(0, F * pieces[w][1], drain, 0)

    def drain_parts(i, _):
        s, c = i // ND, lax.rem(i, ND)
        swap2(0, s, c).wait_send()
        for k in range(2, T, 2):
            part2(s, c, k).wait_send()
        if off:
            @pl.when(helper)
            def _():
                swap2(1, s, c).wait_send()
                for k in range(0, T, 2):
                    part3(s, c, k).wait_send()
        return 0

    @pl.when(mid_plane)
    def _():
        lax.fori_loop(0, F * ND, drain_parts, 0)
        gather_drain(own_rows, sems2)
        if off:
            @pl.when(helper)
            def _():
                gather_drain(end_rows, sems3)
    if off:
        @pl.when(end)
        def _():
            end_copy().wait_send()
    gather_drain(g1, sems1)
    for j in range(4):
        swap1(j).wait_send()
    for k in range(2, T, 2):
        part1(k).wait_send()


def local_layer(sizes, tokens, mix_in, scale, mix_out, up_w, down_w, gains):
    G, F, T = sizes
    R, D = tokens.shape
    K, PWt = mix_in.shape
    Ht = up_w.shape[1]
    NU = max(1, min(4, Ht // 256))
    ND = max(1, min(4, K // 128))
    dims = (G, F, T, R, D, K, PWt, Ht, NU, ND)
    NP = 2 + NU + ND
    H = T // 2
    vmem, hbm = pl.BlockSpec(memory_space=pltpu.VMEM), pl.BlockSpec(memory_space=pl.ANY)
    bf, dma = jnp.bfloat16, pltpu.SemaphoreType.DMA
    return pl.pallas_call(
        functools.partial(kernel, dims),
        out_shape=jax.ShapeDtypeStruct((R, D), bf),
        in_specs=[vmem, vmem, vmem, hbm, hbm, hbm, hbm],
        out_specs=vmem,
        scratch_shapes=[
            pltpu.VMEM((D, PWt), bf), pltpu.VMEM((PWt, D), bf),
            pltpu.VMEM((D, Ht), bf), pltpu.VMEM((Ht, D), bf),
            pltpu.VMEM((T, R, D), bf), pltpu.VMEM((2, T, R, D), bf),
            pltpu.VMEM((2, T * R, Ht), bf),
            pltpu.VMEM((2, H, R, D), bf), pltpu.VMEM((H, R, D), bf), pltpu.VMEM((H - 1, R, D), bf),
            pltpu.VMEM((2, 2, H, R, D), bf), pltpu.VMEM((2, H, R, D), bf), pltpu.VMEM((H, R, D), bf),
            pltpu.VMEM((R, D), bf),
            dma((4,)), dma((F, NP)), dma((F, NP)), dma((F, NP)),
            dma((G - 1, F, NP)), dma((G - 1, F, NP)),
            dma((2, T)), dma((T,)), dma((2, T)), dma((T,)), dma((2, T)), dma((T,)),
            dma((1,)), dma((1,)),
            dma((4,)), dma((4,)), dma((2, F, ND)), dma((2, F, ND)),
            dma((H - 1,)), dma((H - 1,)),
            dma((H - 1, F, ND)), dma((H, F, ND)), dma((H, F, ND)),
        ],
        compiler_params=pltpu.CompilerParams(
            collective_id=0, has_side_effects=True, vmem_limit_bytes=63 * 1024 * 1024),
    )(tokens, gains, scale.reshape(1, PWt), mix_in, mix_out, up_w, down_w)


def solution(mesh):
    sizes = tuple(mesh.shape[name] for name in ("grp", "fs", "tp"))
    return jax.shard_map(
        functools.partial(local_layer, sizes),
        mesh=mesh,
        in_specs=(
            P(("grp", "fs", "tp"), None),
            P("fs", "tp"),
            P("tp"),
            P("tp", "fs"),
            P("fs", "tp"),
            P("tp", "fs"),
            P(),
        ),
        out_specs=P(("grp", "fs", "tp"), None),
        check_vma=False,
    )
```

profile of v0, /device:TPU:0, one launch (start us, length us, event | category | flops | bytes accessed | tf_op | source)
XLA Modules:
  0.0 143.9 jit_solution(14558687697773097700)
XLA Ops:
  0.0 142.0 %shard_map.73 = bf16[128,2048]{1,0:T(8,128)(2,1)} custom-call(bf16[128,2048]{1,0:T(8,128)(2,1)} %tok.1, f32[4,2048]{1,0:T(4,128)} %gains.1, f32[1,256]{1,0:T(1,128)} %bitcast.1, bf16[512,256]{1,0:T(8,128)(2,1)} %mi_h.1, bf16[256,512]{1,0:T(8,128)(2,1)} %mo_h.1, bf16[512,2048]{1,0:T(8,128)(2,1)} %up_h.1, bf16[2048,512]{1,0:T(8,128)(2,1)} %dn_h.1), custom_call_target="tpu_custom_call" | custom-call | tf_op jit(solution)/shard_map/pallas_call | solution.py:541
  142.0 1.9 %copy.9 = bf16[128,2048]{1,0:T(8,128)(2,1)} copy(bf16[128,2048]{1,0:T(8,128)(2,1)} %shard_map.73) | data formatting | bytes 1048576
where the time goes:
time: 144 us
  Pallas kernels  142 us (99%)
  local copies, waits for them, and re-layouts  1.88 us (1%)
    pallas_call x1, Pallas kernels, local_layer(): pl.pallas_call(functools.partial(kernel, dims), out_shape=jax.ShapeDtypeS...  142 us

commit v1 on v0

--- a/solution.py
+++ b/solution.py
@@ -32,9 +32,9 @@
     return average - upcast
 
 
-def kernel(dims, tok, gains, scale, mi_h, mo_h, up_h, dn_h, out,
-           mi, mo, up, dn, g1, g2, hid, sp1, rq1, rp1, sp2, rq2, rp2, mid,
-           lsem, zs_r, zs_l, zr, ys, yr, g1s, g1r, g2s, g2r, g3s, g3r, es, er,
+def kernel(dims, tok_h, gains_h, scale_h, mi_h, mo_h, up_h, dn_h, out,
+           tok, gains, scale, mi, mo, up, dn, g1, g2, hid, sp1, rq1, rp1, sp2, rq2, rp2, mid,
+           lsem, zs, zr, ys, yr, gs, g1r, g2r, g3r, es, er,
            w1s, w1r, w2s, w2r, p1s, p1r, p2s, p2r, p3s):
     G, F, T, R, D, K, PWt, Ht, NU, ND = dims
     g, f, t = lax.axis_index("grp"), lax.axis_index("fs"), lax.axis_index("tp")
@@ -60,6 +60,7 @@
     def shared(w, s):
         return True if w in ("mi", "mo") or not off else ~(helper & (s == helped))
     pieces = {"mi": (0, 1), "mo": (1, 1), "up": (2, NU), "dn": (2 + NU, ND)}
+    kinds = {"mi": 0, "mo": 0, "up": 1, "dn": 1}
     bufs = {"mi": (mi_h, mi), "mo": (mo_h, mo), "up": (up_h, up), "dn": (dn_h, dn)}
 
     def mult(value, by):
@@ -82,9 +83,9 @@
         p = pieces[w][0] + c
         src = bufs[w][0].at[span(w, None, c, g)] if own else view(w, s, c, g)
         target = f + 1 if to_right else f - 1
-        sems = zs_r if to_right else zs_l
-        return pltpu.make_async_remote_copy(
-            src_ref=src, dst_ref=view(w, s, c, g), send_sem=sems.at[s, p], recv_sem=zr.at[s, p],
+        side = 0 if to_right else 1
+        return pltpu.make_async_remote_copy(
+            src_ref=src, dst_ref=view(w, s, c, g), send_sem=zs.at[side, kinds[w], s], recv_sem=zr.at[s, p],
             device_id=(g, target, t), device_id_type=MESH)
 
     def y_copy(w, s, c, k, half=None):
@@ -92,7 +93,7 @@
         half = g if half is None else half
         return pltpu.make_async_remote_copy(
             src_ref=view(w, s, c, half), dst_ref=view(w, s, c, half),
-            send_sem=ys.at[k - 1, s, p], recv_sem=yr.at[k - 1, s, p],
+            send_sem=ys.at[k - 1, kinds[w], s], recv_sem=yr.at[k - 1, s, p],
             device_id=(lax.rem(g + k, G), f, t), device_id_type=MESH)
 
     def send_own(w, c):
@@ -109,7 +110,7 @@
         half = lax.rem(g - k + G, G)
         return pltpu.make_async_remote_copy(
             src_ref=bufs[w][0].at[span(w, None, c, half)], dst_ref=view(w, f, c, half),
-            send_sem=ys.at[k - 1, f, p], recv_sem=yr.at[k - 1, f, p],
+            send_sem=ys.at[k - 1, kinds[w], f], recv_sem=yr.at[k - 1, f, p],
             device_id=(g, inner, t), device_id_type=MESH)
 
     def send_whole(w):
@@ -168,34 +169,33 @@
             src_ref=src, dst_ref=dst, send_sem=send, recv_sem=recv,
             device_id=(g, f, peer(k)), device_id_type=MESH)
 
-    def gather_copy(buf, sems, block, target, row, index):
-        return pltpu.make_async_remote_copy(
-            src_ref=buf.at[block], dst_ref=buf.at[block], send_sem=sems[0].at[row, index],
+    def gather_copy(buf, sems, block, target):
+        return pltpu.make_async_remote_copy(
+            src_ref=buf.at[block], dst_ref=buf.at[block], send_sem=gs.at[sems[0]],
             recv_sem=sems[1].at[block], device_id=(g, f, target), device_id_type=MESH)
 
     def gather_start(buf, sems):
         for k in range(2, T, 2):
-            gather_copy(buf, sems, t, peer(k), 1, peer(k)).start()
-        gather_copy(buf, sems, t, sibling, 0, t).start()
+            gather_copy(buf, sems, t, peer(k)).start()
+        gather_copy(buf, sems, t, sibling).start()
 
     def gather_finish(buf, sems):
         for k in range(2, T, 2):
             block = lax.rem(t - k + T, T)
-            gather_copy(buf, sems, block, sibling, 0, block).wait_recv()
-            gather_copy(buf, sems, block, sibling, 0, block).start()
+            gather_copy(buf, sems, block, sibling).wait_recv()
+            gather_copy(buf, sems, block, sibling).start()
         for k in range(0, T, 2):
             block = lax.rem(sibling - k + T, T)
-            gather_copy(buf, sems, block, sibling, 0, block).wait_recv()
+            gather_copy(buf, sems, block, sibling).wait_recv()
 
     def gather_drain(buf, sems):
-        for k in range(2, T, 2):
-            gather_copy(buf, sems, t, peer(k), 1, peer(k)).wait_send()
-        for k in range(0, T, 2):
-            block = lax.rem(t - k + T, T)
-            gather_copy(buf, sems, block, sibling, 0, block).wait_send()
+        sent = buf.at[pl.ds(0, T - 1)]
+        pltpu.make_async_remote_copy(
+            src_ref=sent, dst_ref=sent, send_sem=gs.at[sems[0]], recv_sem=sems[1].at[0],
+            device_id=(g, f, sibling), device_id_type=MESH).wait_send()
 
     own_rows, end_rows = g2.at[0], g2.at[1]
-    sems1, sems2, sems3 = (g1s, g1r), (g2s, g2r), (g3s, g3r)
+    sems1, sems2, sems3 = (0, g1r), (1, g2r), (2, g3r)
 
     def end_copy():
         return pltpu.make_async_remote_copy(
@@ -206,7 +206,7 @@
         cols = pl.ds(j * step, step)
         return pltpu.make_async_remote_copy(
             src_ref=sp1.at[1 - place, :, :, cols], dst_ref=rq1.at[:, :, cols],
-            send_sem=w1s.at[j], recv_sem=w1r.at[j], device_id=(g, f, sibling), device_id_type=MESH)
+            send_sem=w1s.at[0], recv_sem=w1r.at[j], device_id=(g, f, sibling), device_id_type=MESH)
 
     def part1(k):
         return tp_copy(sp1.at[place, peer(k) // 2], rp1.at[k // 2 - 1],
@@ -218,21 +218,28 @@
     def swap2(i, s, c):
         return pltpu.make_async_remote_copy(
             src_ref=sp2.at[i, 1 - place, :, :, columns(s, c)], dst_ref=rq2.at[i, :, :, columns(s, c)],
-            send_sem=w2s.at[i, s, c], recv_sem=w2r.at[i, s, c],
+            send_sem=w2s.at[i], recv_sem=w2r.at[i, s, c],
             device_id=(g, f, sibling), device_id_type=MESH)
 
     def part2(s, c, k):
         return tp_copy(sp2.at[0, place, peer(k) // 2, :, columns(s, c)], rp2.at[k // 2, :, columns(s, c)],
-                       p2s.at[k // 2 - 1, s, c], p2r.at[k // 2, s, c], k)
+                       p2s.at[k // 2 - 1], p2r.at[k // 2], k)
 
     def part3(s, c, k):
         return pltpu.make_async_remote_copy(
             src_ref=sp2.at[1, place, peer(k) // 2, :, columns(s, c)], dst_ref=rp2.at[k // 2, :, columns(s, c)],
-            send_sem=p3s.at[k // 2, s, c], recv_sem=p2r.at[k // 2, s, c],
+            send_sem=p3s.at[k // 2], recv_sem=p2r.at[k // 2],
             device_id=(g, helped, peer(k)), device_id_type=MESH)
 
     def merge(a, b):
         return (a.astype(jnp.float32) + b.astype(jnp.float32)).astype(jnp.bfloat16)
+
+    loads = [pltpu.make_async_copy(a, b, lsem.at[4 + i])
+             for i, (a, b) in enumerate(((tok_h, tok), (gains_h, gains), (scale_h, scale)))]
+    for load in loads:
+        load.start()
+    for index, w in enumerate(("mi", "mo", "up", "dn")):
+        local(w, index).start()
 
     barrier = pltpu.get_barrier_semaphore()
 
@@ -265,9 +272,8 @@
     send_own("mi", 0)
     send_own("mo", 0)
     send_own("up", 0)
-    for index, w in enumerate(("mi", "mo", "up", "dn")):
-        local(w, index).start()
-
+    for load in loads:
+        load.wait()
     g1[t] = normalize(tok[...], gains[0:1, :]).astype(jnp.bfloat16)
     gather_start(g1, sems1)
 
@@ -448,16 +454,15 @@
     def _():
         lax.fori_loop(ND, (far + 1) * ND + 2, dn_step, 0)
 
-    def take(i, _):
-        s, c = i // ND, lax.rem(i, ND)
-        for k in range(2, T, 2):
-            part2(s, c, k).wait_recv()
-        if off:
-            @pl.when(end)
-            def _():
-                part3(s, c, 0).wait_recv()
-        return 0
-    lax.fori_loop(0, F * ND, take, 0)
+    def landed(k):
+        return tp_copy(rp2.at[k // 2], rp2.at[k // 2], p2s.at[0], p2r.at[k // 2], 2)
+
+    for k in range(2, T, 2):
+        landed(k).wait_recv()
+    if off:
+        @pl.when(end)
+        def _():
+            landed(0).wait_recv()
 
     @pl.when(mid_plane)
     def _():
@@ -468,60 +473,60 @@
     channel_out = total.astype(jnp.bfloat16)
     out[...] = (mid[...].astype(jnp.float32) + normalize(channel_out, gains[3:4, :])).astype(jnp.bfloat16)
 
-    for w in ("mi", "mo", "up", "dn"):
-        def drain(i, _):
-            s, c = i // pieces[w][1], lax.rem(i, pieces[w][1])
-
-            moved = True if w in ("mi", "mo") else (mid_plane | (s == f))
+    def sent(kind, sem):
+        rows = (mi if kind == 0 else up).at[pl.ds(0, 2 * (K // G)), :]
+        pltpu.make_async_remote_copy(
+            src_ref=rows, dst_ref=rows, send_sem=sem, recv_sem=zr.at[0, 0],
+            device_id=(g, f, sibling), device_id_type=MESH).wait_send()
+
+    for kind, w in ((0, "mi"), (1, "up")):
+        def drain(s, _):
+            moved = True if kind == 0 else (mid_plane | (s == f))
 
             @pl.when((s <= f) & to_right_ok(w) & moved)
             def _():
-                z_copy(w, s, c, True).wait_send()
+                sent(kind, zs.at[0, kind, s])
 
             @pl.when((s >= f) & to_left_ok(w) & moved)
             def _():
-                z_copy(w, s, c, False).wait_send()
+                sent(kind, zs.at[1, kind, s])
 
             @pl.when((s != f) & moved & shared(w, s))
             def _():
                 for k in range(1, G):
-                    y_copy(w, s, c, k).wait_send()
-            if off and w in ("up", "dn"):
+                    sent(kind, ys.at[k - 1, kind, s])
+            if off and kind == 1:
                 @pl.when((s == f) & end)
                 def _():
                     for k in range(1, G):
-                        whole_copy(w, c, k).wait_send()
+                        sent(kind, ys.at[k - 1, kind, s])
             return 0
-        lax.fori_loop(0, F * pieces[w][1], drain, 0)
-
-    def drain_parts(i, _):
-        s, c = i // ND, lax.rem(i, ND)
-        swap2(0, s, c).wait_send()
+        lax.fori_loop(0, F, drain, 0)
+
+    def swapped(buf, sem):
+        pltpu.make_async_remote_copy(
+            src_ref=buf, dst_ref=buf, send_sem=sem, recv_sem=w1r.at[0],
+            device_id=(g, f, sibling), device_id_type=MESH).wait_send()
+
+    @pl.when(mid_plane)
+    def _():
+        swapped(rq2.at[0], w2s.at[0])
         for k in range(2, T, 2):
-            part2(s, c, k).wait_send()
-        if off:
-            @pl.when(helper)
-            def _():
-                swap2(1, s, c).wait_send()
-                for k in range(0, T, 2):
-                    part3(s, c, k).wait_send()
-        return 0
-
-    @pl.when(mid_plane)
-    def _():
-        lax.fori_loop(0, F * ND, drain_parts, 0)
+            swapped(rp2.at[0], p2s.at[k // 2 - 1])
         gather_drain(own_rows, sems2)
         if off:
             @pl.when(helper)
             def _():
                 gather_drain(end_rows, sems3)
+                swapped(rq2.at[1], w2s.at[1])
+                for k in range(0, T, 2):
+                    swapped(rp2.at[0], p3s.at[k // 2])
     if off:
         @pl.when(end)
         def _():
             end_copy().wait_send()
     gather_drain(g1, sems1)
-    for j in range(4):
-        swap1(j).wait_send()
+    swapped(rq1, w1s.at[0])
     for k in range(2, T, 2):
         part1(k).wait_send()
 
@@ -540,10 +545,11 @@
     bf, dma = jnp.bfloat16, pltpu.SemaphoreType.DMA
     return pl.pallas_call(
         functools.partial(kernel, dims),
-        out_shape=jax.ShapeDtypeStruct((R, D), bf),
-        in_specs=[vmem, vmem, vmem, hbm, hbm, hbm, hbm],
+        out_shape=pltpu.VMEM((R, D), bf),
+        in_specs=[hbm] * 7,
         out_specs=vmem,
         scratch_shapes=[
+            pltpu.VMEM((R, D), bf), pltpu.VMEM(gains.shape, jnp.float32), pltpu.VMEM((1, PWt), jnp.float32),
             pltpu.VMEM((D, PWt), bf), pltpu.VMEM((PWt, D), bf),
             pltpu.VMEM((D, Ht), bf), pltpu.VMEM((Ht, D), bf),
             pltpu.VMEM((T, R, D), bf), pltpu.VMEM((2, T, R, D), bf),
@@ -551,13 +557,13 @@
             pltpu.VMEM((2, H, R, D), bf), pltpu.VMEM((H, R, D), bf), pltpu.VMEM((H - 1, R, D), bf),
             pltpu.VMEM((2, 2, H, R, D), bf), pltpu.VMEM((2, H, R, D), bf), pltpu.VMEM((H, R, D), bf),
             pltpu.VMEM((R, D), bf),
-            dma((4,)), dma((F, NP)), dma((F, NP)), dma((F, NP)),
-            dma((G - 1, F, NP)), dma((G - 1, F, NP)),
-            dma((2, T)), dma((T,)), dma((2, T)), dma((T,)), dma((2, T)), dma((T,)),
+            dma((7,)), dma((2, 2, F)), dma((F, NP)),
+            dma((G - 1, 2, F)), dma((G - 1, F, NP)),
+            dma((3,)), dma((T,)), dma((T,)), dma((T,)),
             dma((1,)), dma((1,)),
-            dma((4,)), dma((4,)), dma((2, F, ND)), dma((2, F, ND)),
+            dma((1,)), dma((4,)), dma((2,)), dma((2, F, ND)),
             dma((H - 1,)), dma((H - 1,)),
-            dma((H - 1, F, ND)), dma((H, F, ND)), dma((H, F, ND)),
+            dma((H - 1,)), dma((H,)), dma((H,)),
         ],
         compiler_params=pltpu.CompilerParams(
             collective_id=0, has_side_effects=True, vmem_limit_bytes=63 * 1024 * 1024),

time: 144 us -> 138 us (0.958)
  Pallas kernels: 142 us -> 137 us
    pallas_call x1, Pallas kernels: 142 us -> 137 us  [local_layer(): pl.pallas_call(functools.partial(kernel, dims), out_shape=pltpu.VMEM((R,...]
where the time goes in v1:
time: 138 us
  Pallas kernels  137 us (99%)
    pallas_call x1, Pallas kernels, local_layer(): pl.pallas_call(functools.partial(kernel, dims), out_shape=pltpu.VMEM((R,...  137 us

profile of v1, /device:TPU:0, one launch (start us, length us, event | category | flops | bytes accessed | tf_op | source)
XLA Modules:
  0.0 138.0 jit_solution(10782638275947685331)
XLA Ops:
  0.0 137.2 %shard_map.73 = bf16[128,2048]{1,0:T(8,128)(2,1)S(1)} custom-call(bf16[128,2048]{1,0:T(8,128)(2,1)} %tok_h.1, f32[4,2048]{1,0:T(4,128)} %gains_h.1, f32[1,256]{1,0:T(1,128)} %bitcast.1, bf16[512,256]{1,0:T(8,128)(2,1)} %mi_h.1, bf16[256,512]{1,0:T(8,128)(2,1)} %mo_h.1, bf16[512,2048]{1,0:T(8,128)(2,1)} %up_h.1, bf16[2048,512]{1,0:T(8,128)(2,1)} %dn_h.1), custom_call_target="tpu_custom_call" | custom-call | tf_op jit(solution)/shard_map/pallas_call | solution.py:546
  137.2 0.8 copy.9

commit v2 on v1

--- a/solution.py
+++ b/solution.py
@@ -39,6 +39,9 @@
     G, F, T, R, D, K, PWt, Ht, NU, ND = dims
     g, f, t = lax.axis_index("grp"), lax.axis_index("fs"), lax.axis_index("tp")
     cu, cd = Ht // NU, K // ND
+    UD = 1 if ND % 2 else 2
+    NB = ND // UD
+    cw = UD * cd
     off = F >= 4
     far = F - 2 if off else F - 1
     first, last = (1, F - 2) if off else (0, F - 1)
@@ -212,22 +215,22 @@
         return tp_copy(sp1.at[place, peer(k) // 2], rp1.at[k // 2 - 1],
                        p1s.at[k // 2 - 1], p1r.at[k // 2 - 1], k)
 
-    def columns(s, c):
-        return pl.ds(mult(s * K + c * cd, cd), cd)
-
-    def swap2(i, s, c):
-        return pltpu.make_async_remote_copy(
-            src_ref=sp2.at[i, 1 - place, :, :, columns(s, c)], dst_ref=rq2.at[i, :, :, columns(s, c)],
-            send_sem=w2s.at[i], recv_sem=w2r.at[i, s, c],
+    def columns(s, u):
+        return pl.ds(mult(s * K + u * cw, cw), cw)
+
+    def swap2(i, s, u):
+        return pltpu.make_async_remote_copy(
+            src_ref=sp2.at[i, 1 - place, :, :, columns(s, u)], dst_ref=rq2.at[i, :, :, columns(s, u)],
+            send_sem=w2s.at[i], recv_sem=w2r.at[i, s, u],
             device_id=(g, f, sibling), device_id_type=MESH)
 
-    def part2(s, c, k):
-        return tp_copy(sp2.at[0, place, peer(k) // 2, :, columns(s, c)], rp2.at[k // 2, :, columns(s, c)],
+    def part2(s, u, k):
+        return tp_copy(sp2.at[0, place, peer(k) // 2, :, columns(s, u)], rp2.at[k // 2, :, columns(s, u)],
                        p2s.at[k // 2 - 1], p2r.at[k // 2], k)
 
-    def part3(s, c, k):
-        return pltpu.make_async_remote_copy(
-            src_ref=sp2.at[1, place, peer(k) // 2, :, columns(s, c)], dst_ref=rp2.at[k // 2, :, columns(s, c)],
+    def part3(s, u, k):
+        return pltpu.make_async_remote_copy(
+            src_ref=sp2.at[1, place, peer(k) // 2, :, columns(s, u)], dst_ref=rp2.at[k // 2, :, columns(s, u)],
             send_sem=p3s.at[k // 2], recv_sem=p2r.at[k // 2],
             device_id=(g, helped, peer(k)), device_id_type=MESH)
 
@@ -355,104 +358,127 @@
     if far > 1:
         pump_all("up", far)
 
-    width = 256
-
-    def up_project(i):
-        def up_step(j, _):
-            cols = pl.ds(mult(j * width, width), width)
-            pre = jnp.dot(g2[i].reshape(T * R, D), up[:, cols], preferred_element_type=jnp.float32)
-            pre = jnp.maximum(pre, 0.0)
-            hid[i, :, cols] = (pre * pre).astype(jnp.bfloat16)
-            return 0
-        lax.fori_loop(0, Ht // width, up_step, 0)
+    def up_project(i, c):
+        cols = pl.ds(mult(c * cu, cu), cu)
+        pre = jnp.dot(g2[i].reshape(T * R, D), up[:, cols], preferred_element_type=jnp.float32)
+        pre = jnp.maximum(pre, 0.0)
+        hid[i, :, cols] = (pre * pre).astype(jnp.bfloat16)
+
+    half_u, half_d = NU // 2, (ND + 1) // 2
+    turn = max(half_u - 1, 0)
+    soon = [c for c in range(half_d) if half_u + c < NU]
+    if off and half_d < ND:
+        soon.append(half_d)
+    later = [c for c in range(ND) if c not in soon]
+
+    def up_step(j, _):
+        i, c = j // NU, lax.rem(j, NU)
+
+        @pl.when(i == 0)
+        def _():
+            def landed_rows(s, _):
+                @pl.when(s != f)
+                def _():
+                    y_wait("up", s, c)
+                return 0
+            lax.fori_loop(0, F, landed_rows, 0)
+        if off:
+            @pl.when(helper & (i == 1) & (c == 0))
+            def _():
+                gather_finish(end_rows, sems3)
+
+        @pl.when((i == 0) | helper)
+        def _():
+            up_project(i, c)
+        if off:
+            @pl.when(helper & (i == 0) & (c == turn))
+            def _():
+                end_copy().wait_recv()
+                gather_start(end_rows, sems3)
+        first_pass = (i == 0) & (c >= half_u) & (c - half_u < half_d)
+        second_pass = (i == 1) & (c == turn) & (half_d < ND)
+
+        @pl.when(first_pass | second_pass)
+        def _():
+            pump("dn", 1, jnp.where(i == 0, c - half_u, half_d))
+        return 0
 
     local("up", 2).wait()
     local("dn", 3).wait()
 
-    @pl.when(mid_plane)
-    def _():
-        gather_finish(own_rows, sems2)
+    def dn_compute(s, u):
+        @pl.when(s != f)
+        def _():
+            for c in range(UD):
+                y_wait("dn", s, u * UD + c)
+        cols = columns(s, u)
+
+        def project(i):
+            value = jnp.dot(hid[i], dn[:, cols], preferred_element_type=jnp.float32
+                            ).astype(jnp.bfloat16).reshape(half_t, 2, R, cw)
+            for q in range(2):
+                sp2[i, q, :, :, cols] = value[:, q]
+            swap2(i, s, u).start()
         if off:
             @pl.when(helper)
             def _():
-                end_copy().wait_recv()
-                gather_start(end_rows, sems3)
-        y_wait_all("up")
-        up_project(0)
-        for c in range(ND // 2):
-            pump("dn", 1, c)
-        if off:
-            @pl.when(helper)
-            def _():
-                gather_finish(end_rows, sems3)
-                up_project(1)
-
-    def dn_compute(s, c):
-        @pl.when(s != f)
-        def _():
-            y_wait("dn", s, c)
-        cols = columns(s, c)
-
-        def project(i):
-            value = jnp.dot(hid[i], dn[:, cols], preferred_element_type=jnp.float32
-                            ).astype(jnp.bfloat16).reshape(half_t, 2, R, cd)
-            for q in range(2):
-                sp2[i, q, :, :, cols] = value[:, q]
-            swap2(i, s, c).start()
-        if off:
-            @pl.when(helper)
-            def _():
                 project(1)
         project(0)
 
-    def dn_merge(s, c):
-        cols = columns(s, c)
+    def dn_merge(s, u):
+        cols = columns(s, u)
 
         def finish(i):
-            swap2(i, s, c).wait_recv()
+            swap2(i, s, u).wait_recv()
             sp2[i, place, :, :, cols] = merge(sp2[i, place, :, :, cols], rq2[i, :, :, cols])
         if off:
             @pl.when(helper)
             def _():
                 finish(1)
                 for k in range(0, T, 2):
-                    part3(s, c, k).start()
+                    part3(s, u, k).start()
         finish(0)
         for k in range(2, T, 2):
-            part2(s, c, k).start()
-
-    def dn_step(e, _):
-        d, c = e // ND, lax.rem(e, ND)
-
-        @pl.when((d <= far) & (e >= ND + ND // 2))
-        def _():
-            pump("dn", d, c)
-
+            part2(s, u, k).start()
+
+    slots = (far + 1) * NB
+
+    def dn_step(n, _):
         def one(j, _):
-            now = j // 4
-            late = lax.rem(j, 4) // 2
-            side = lax.rem(j, 2)
-            ev = e - 1 + now - ND + late * (ND - 1)
-            dd, cc = ev // ND, lax.rem(ev, ND)
-            s = f + (2 * side - 1) * dd
-            right_turn = jnp.where(late == 1, dd == far, dd < far)
-            once = (dd > 0) | (side == 0)
-            wanted = (ev >= 0) & right_turn & once & (s >= 0) & (s < F)
+            now, which = j // 3, lax.rem(j, 3)
+            slot = n - 1 + now
+            d, u = slot // NB, lax.rem(slot, NB)
+            s = jnp.where(which == 0, helped, jnp.where(which == 1, f - d, f + d))
+            theirs = helper & (s == helped)
+            side = (s >= 0) & (s < F) & ~theirs & ((which == 1) | (d > 0))
+            wanted = (slot >= 0) & (slot < slots) & jnp.where(which == 0, helper & (d == far), side)
 
             @pl.when(wanted & (now == 0))
             def _():
-                dn_merge(s, cc)
+                dn_merge(s, u)
 
             @pl.when(wanted & (now == 1))
             def _():
-                dn_compute(s, cc)
+                dn_compute(s, u)
             return 0
-        lax.fori_loop(0, 8, one, 0)
+        lax.fori_loop(0, 6, one, 0)
+
+        @pl.when(n == NB - 1)
+        def _():
+            for c in later:
+                pump("dn", 1, c)
+
+        @pl.when((n >= NB) & (n < far * NB))
+        def _():
+            for c in range(UD):
+                pump("dn", n // NB + 1, lax.rem(n, NB) * UD + c)
         return 0
 
     @pl.when(mid_plane)
     def _():
-        lax.fori_loop(ND, (far + 1) * ND + 2, dn_step, 0)
+        gather_finish(own_rows, sems2)
+        lax.fori_loop(0, (2 if off else 1) * NU, up_step, 0)
+        lax.fori_loop(0, slots + 1, dn_step, 0)
 
     def landed(k):
         return tp_copy(rp2.at[k // 2], rp2.at[k // 2], p2s.at[0], p2r.at[k // 2], 2)
@@ -561,7 +587,7 @@
             dma((G - 1, 2, F)), dma((G - 1, F, NP)),
             dma((3,)), dma((T,)), dma((T,)), dma((T,)),
             dma((1,)), dma((1,)),
-            dma((1,)), dma((4,)), dma((2,)), dma((2, F, ND)),
+            dma((1,)), dma((4,)), dma((2,)), dma((2, F, ND if ND % 2 else ND // 2)),
             dma((H - 1,)), dma((H - 1,)),
             dma((H - 1,)), dma((H,)), dma((H,)),
         ],

time: 138 us -> 137 us (level)
  no operation moved by 1% of the time
where the time goes in v2:
time: 137 us
  Pallas kernels  136 us (99%)
    pallas_call x1, Pallas kernels, local_layer(): pl.pallas_call(functools.partial(kernel, dims), out_shape=pltpu.VMEM((R,...  136 us

profile of v2, /device:TPU:0, one launch (start us, length us, event | category | flops | bytes accessed | tf_op | source)
XLA Modules:
  0.0 136.7 jit_solution(2640479782342394679)
XLA Ops:
  0.0 135.9 %shard_map.73 = bf16[128,2048]{1,0:T(8,128)(2,1)S(1)} custom-call(bf16[128,2048]{1,0:T(8,128)(2,1)} %tok_h.1, f32[4,2048]{1,0:T(4,128)} %gains_h.1, f32[1,256]{1,0:T(1,128)} %bitcast.1, bf16[512,256]{1,0:T(8,128)(2,1)} %mi_h.1, bf16[256,512]{1,0:T(8,128)(2,1)} %mo_h.1, bf16[512,2048]{1,0:T(8,128)(2,1)} %up_h.1, bf16[2048,512]{1,0:T(8,128)(2,1)} %dn_h.1), custom_call_target="tpu_custom_call" | custom-call | tf_op jit(solution)/shard_map/pallas_call | solution.py:572
  135.9 0.8 copy.9

commit v3 on v2

--- a/solution.py
+++ b/solution.py
@@ -43,6 +43,7 @@
     NB = ND // UD
     cw = UD * cd
     off = F >= 4
+    tuned = F == 4 and NU == 4 and ND == 4
     far = F - 2 if off else F - 1
     first, last = (1, F - 2) if off else (0, F - 1)
     mid_plane = (f >= first) & (f <= last)
@@ -118,19 +119,37 @@
 
     def send_whole(w):
         if off:
+            order = list(range(pieces[w][1]))
+            if tuned and w == "dn":
+                order = order[-1:] + order[:-1]
+
             @pl.when(end)
             def _():
-                for c in range(pieces[w][1]):
+                for c in order:
                     for k in range(1, G):
                         whole_copy(w, c, k).start()
 
-    def pump(w, d, c):
+    def pass_on(k):
+        half = lax.rem(g - k + G, G)
+        p = pieces["dn"][0] + ND - 1
+        block = view("dn", helped, ND - 1, half)
+        return pltpu.make_async_remote_copy(
+            src_ref=block, dst_ref=block, send_sem=ys.at[k - 1, 1, helped], recv_sem=yr.at[k - 1, helped, p],
+            device_id=(g, F - 1 - f, t), device_id_type=MESH)
+
+    def pump(w, d, c, kind=None):
         for to_right in (True, False):
             s = f - d if to_right else f + d
             more = to_right_ok(w) if to_right else to_left_ok(w)
             here = (s >= 0) & (s < F)
             if w in ("up", "dn"):
                 here = here & mid_plane
+            theirs = helper & (s == helped)
+            if kind is not None:
+                here = here & (theirs if kind == "relay" else ~theirs)
+            spread = shared(w, s)
+            if tuned and w == "dn" and c == ND - 1:
+                spread = spread & (s > 0) & (s < F - 1)
 
             @pl.when(here)
             def _():
@@ -140,7 +159,7 @@
                 def _():
                     z_copy(w, s, c, to_right).start()
 
-                @pl.when(shared(w, s))
+                @pl.when(spread)
                 def _():
                     for k in range(1, G):
                         y_copy(w, s, c, k).start()
@@ -371,6 +390,26 @@
         soon.append(half_d)
     later = [c for c in range(ND) if c not in soon]
 
+    def act(todo):
+        for what, d, c in todo:
+            if what == "pass":
+                y_wait("dn", helped, ND - 1)
+                for k in range(1, G):
+                    pass_on(k).start()
+            else:
+                pump("dn", d, c, what)
+
+    up_acts = {2: [("near", 1, 0)], 3: [("near", 1, 1), ("relay", 1, 0), ("near", 1, 2)], 5: [("relay", 1, 1)],
+               6: [("near", 1, 3)], 7: [("relay", 1, 2)]}
+    dn_acts = {3: [("relay", 1, 3), ("near", 2, 0)], 5: [("near", 2, 1)], 7: [("near", 2, 2), ("pass", 0, 0)],
+               8: [("near", 2, 3)]}
+
+    def scheduled(acts, n):
+        for index, todo in acts.items():
+            @pl.when(n == index)
+            def _():
+                act(todo)
+
     def up_step(j, _):
         i, c = j // NU, lax.rem(j, NU)
 
@@ -395,6 +434,9 @@
             def _():
                 end_copy().wait_recv()
                 gather_start(end_rows, sems3)
+        if tuned:
+            scheduled(up_acts, j)
+            return 0
         first_pass = (i == 0) & (c >= half_u) & (c - half_u < half_d)
         second_pass = (i == 1) & (c == turn) & (half_d < ND)
 
@@ -410,7 +452,12 @@
         @pl.when(s != f)
         def _():
             for c in range(UD):
-                y_wait("dn", s, u * UD + c)
+                if tuned and c == UD - 1:
+                    @pl.when(~(helper & (s == helped) & (u == NB - 1)))
+                    def _():
+                        y_wait("dn", s, u * UD + c)
+                else:
+                    y_wait("dn", s, u * UD + c)
         cols = columns(s, u)
 
         def project(i):
@@ -444,14 +491,15 @@
     slots = (far + 1) * NB
 
     def dn_step(n, _):
-        def one(j, _):
-            now, which = j // 3, lax.rem(j, 3)
-            slot = n - 1 + now
+        def one(now, _):
+            m = n - 1 + now
+            slot, q = m // 2, lax.rem(m, 2)
             d, u = slot // NB, lax.rem(slot, NB)
-            s = jnp.where(which == 0, helped, jnp.where(which == 1, f - d, f + d))
-            theirs = helper & (s == helped)
-            side = (s >= 0) & (s < F) & ~theirs & ((which == 1) | (d > 0))
-            wanted = (slot >= 0) & (slot < slots) & jnp.where(which == 0, helper & (d == far), side)
+            last = helper & (d == far)
+            s = jnp.where(q == 0, f - d, f + d)
+            s = jnp.where(last, jnp.where(q == 0, F - 1 - helped, helped), s)
+            wanted = ((m >= 0) & (slot < slots) & (s >= 0) & (s < F) & ((q == 0) | (d > 0))
+                      & (last | ~(helper & (s == helped))))
 
             @pl.when(wanted & (now == 0))
             def _():
@@ -461,24 +509,28 @@
             def _():
                 dn_compute(s, u)
             return 0
-        lax.fori_loop(0, 6, one, 0)
-
-        @pl.when(n == NB - 1)
+        lax.fori_loop(0, 2, one, 0)
+        if tuned:
+            scheduled(dn_acts, n)
+            return 0
+        slot = n // 2
+
+        @pl.when(n == 2 * NB - 1)
         def _():
             for c in later:
                 pump("dn", 1, c)
 
-        @pl.when((n >= NB) & (n < far * NB))
+        @pl.when((lax.rem(n, 2) == 1) & (slot >= NB) & (slot < far * NB))
         def _():
             for c in range(UD):
-                pump("dn", n // NB + 1, lax.rem(n, NB) * UD + c)
+                pump("dn", slot // NB + 1, lax.rem(slot, NB) * UD + c)
         return 0
 
     @pl.when(mid_plane)
     def _():
         gather_finish(own_rows, sems2)
         lax.fori_loop(0, (2 if off else 1) * NU, up_step, 0)
-        lax.fori_loop(0, slots + 1, dn_step, 0)
+        lax.fori_loop(0, 2 * slots + 1, dn_step, 0)
 
     def landed(k):
         return tp_copy(rp2.at[k // 2], rp2.at[k // 2], p2s.at[0], p2r.at[k // 2], 2)
@@ -505,6 +557,11 @@
             src_ref=rows, dst_ref=rows, send_sem=sem, recv_sem=zr.at[0, 0],
             device_id=(g, f, sibling), device_id_type=MESH).wait_send()
 
+    def swapped(buf, sem):
+        pltpu.make_async_remote_copy(
+            src_ref=buf, dst_ref=buf, send_sem=sem, recv_sem=w1r.at[0],
+            device_id=(g, f, sibling), device_id_type=MESH).wait_send()
+
     for kind, w in ((0, "mi"), (1, "up")):
         def drain(s, _):
             moved = True if kind == 0 else (mid_plane | (s == f))
@@ -517,10 +574,23 @@
             def _():
                 sent(kind, zs.at[1, kind, s])
 
-            @pl.when((s != f) & moved & shared(w, s))
+            gone = (s != f) & moved & shared(w, s)
+            ends = (s == 0) | (s == F - 1) if tuned and kind == 1 else s < 0
+
+            @pl.when(gone & ~ends)
             def _():
                 for k in range(1, G):
                     sent(kind, ys.at[k - 1, kind, s])
+            if tuned and kind == 1:
+                @pl.when(gone & ends)
+                def _():
+                    for k in range(1, G):
+                        swapped(up.at[pl.ds(0, 2 * (K // G) - cd // G), :], ys.at[k - 1, kind, s])
+
+                @pl.when(helper & (s == helped))
+                def _():
+                    for k in range(1, G):
+                        swapped(view("dn", 0, 0, 0), ys.at[k - 1, kind, s])
             if off and kind == 1:
                 @pl.when((s == f) & end)
                 def _():
@@ -528,11 +598,6 @@
                         sent(kind, ys.at[k - 1, kind, s])
             return 0
         lax.fori_loop(0, F, drain, 0)
-
-    def swapped(buf, sem):
-        pltpu.make_async_remote_copy(
-            src_ref=buf, dst_ref=buf, send_sem=sem, recv_sem=w1r.at[0],
-            device_id=(g, f, sibling), device_id_type=MESH).wait_send()
 
     @pl.when(mid_plane)
     def _():

time: 137 us -> 127 us (0.927)
  Pallas kernels: 136 us -> 126 us
    pallas_call x1, Pallas kernels: 136 us -> 126 us  [local_layer(): pl.pallas_call(functools.partial(kernel, dims), out_shape=pltpu.VMEM((R,...]
where the time goes in v3:
time: 127 us; the launch traced here: 126 us
  Pallas kernels  126 us (99%)
    pallas_call x1, Pallas kernels, local_layer(): pl.pallas_call(functools.partial(kernel, dims), out_shape=pltpu.VMEM((R,...  126 us

profile of v3, /device:TPU:0, one launch (start us, length us, event | category | flops | bytes accessed | tf_op | source)
XLA Modules:
  0.0 126.5 jit_solution(5142113732489863973)
XLA Ops:
  0.0 125.7 %shard_map.73 = bf16[128,2048]{1,0:T(8,128)(2,1)S(1)} custom-call(bf16[128,2048]{1,0:T(8,128)(2,1)} %tok_h.1, f32[4,2048]{1,0:T(4,128)} %gains_h.1, f32[1,256]{1,0:T(1,128)} %bitcast.1, bf16[512,256]{1,0:T(8,128)(2,1)} %mi_h.1, bf16[256,512]{1,0:T(8,128)(2,1)} %mo_h.1, bf16[512,2048]{1,0:T(8,128)(2,1)} %up_h.1, bf16[2048,512]{1,0:T(8,128)(2,1)} %dn_h.1), custom_call_target="tpu_custom_call" | custom-call | tf_op jit(solution)/shard_map/pallas_call | solution.py:637
  125.7 0.8 copy.9

commit v4 on v3

--- a/solution.py
+++ b/solution.py
@@ -41,7 +41,6 @@
     cu, cd = Ht // NU, K // ND
     UD = 1 if ND % 2 else 2
     NB = ND // UD
-    cw = UD * cd
     off = F >= 4
     tuned = F == 4 and NU == 4 and ND == 4
     far = F - 2 if off else F - 1
@@ -71,7 +70,7 @@
         return pl.multiple_of(value, by)
 
     def span(w, s, c, half):
-        base = 0 if s is None else s * K
+        base = s * K
         if w == "mi":
             return pl.ds(mult(base + half * (K // G), K // G), K // G), pl.ds(0, PWt)
         if w == "mo":
@@ -83,13 +82,12 @@
     def view(w, s, c, half):
         return bufs[w][1].at[span(w, s, c, half)]
 
-    def z_copy(w, s, c, to_right, own=False):
+    def z_copy(w, s, c, to_right):
         p = pieces[w][0] + c
-        src = bufs[w][0].at[span(w, None, c, g)] if own else view(w, s, c, g)
         target = f + 1 if to_right else f - 1
         side = 0 if to_right else 1
         return pltpu.make_async_remote_copy(
-            src_ref=src, dst_ref=view(w, s, c, g), send_sem=zs.at[side, kinds[w], s], recv_sem=zr.at[s, p],
+            src_ref=view(w, s, c, g), dst_ref=view(w, s, c, g), send_sem=zs.at[side, kinds[w], s], recv_sem=zr.at[s, p],
             device_id=(g, target, t), device_id_type=MESH)
 
     def y_copy(w, s, c, k, half=None):
@@ -103,17 +101,17 @@
     def send_own(w, c):
         @pl.when(to_right_ok(w))
         def _():
-            z_copy(w, f, c, True, own=True).start()
+            z_copy(w, f, c, True).start()
 
         @pl.when(to_left_ok(w))
         def _():
-            z_copy(w, f, c, False, own=True).start()
+            z_copy(w, f, c, False).start()
 
     def whole_copy(w, c, k):
         p = pieces[w][0] + c
         half = lax.rem(g - k + G, G)
         return pltpu.make_async_remote_copy(
-            src_ref=bufs[w][0].at[span(w, None, c, half)], dst_ref=view(w, f, c, half),
+            src_ref=view(w, f, c, half), dst_ref=view(w, f, c, half),
             send_sem=ys.at[k - 1, kinds[w], f], recv_sem=yr.at[k - 1, f, p],
             device_id=(g, inner, t), device_id_type=MESH)
 
@@ -121,7 +119,7 @@
         if off:
             order = list(range(pieces[w][1]))
             if tuned and w == "dn":
-                order = order[-1:] + order[:-1]
+                order = order[:1:-1] + order[:2]
 
             @pl.when(end)
             def _():
@@ -234,22 +232,22 @@
         return tp_copy(sp1.at[place, peer(k) // 2], rp1.at[k // 2 - 1],
                        p1s.at[k // 2 - 1], p1r.at[k // 2 - 1], k)
 
-    def columns(s, u):
-        return pl.ds(mult(s * K + u * cw, cw), cw)
-
-    def swap2(i, s, u):
-        return pltpu.make_async_remote_copy(
-            src_ref=sp2.at[i, 1 - place, :, :, columns(s, u)], dst_ref=rq2.at[i, :, :, columns(s, u)],
-            send_sem=w2s.at[i], recv_sem=w2r.at[i, s, u],
+    def columns(s, c, n):
+        return pl.ds(mult(s * K + c * cd, cd), n * cd)
+
+    def swap2(i, s, c, n):
+        return pltpu.make_async_remote_copy(
+            src_ref=sp2.at[i, 1 - place, :, :, columns(s, c, n)], dst_ref=rq2.at[i, :, :, columns(s, c, n)],
+            send_sem=w2s.at[i], recv_sem=w2r.at[i, s, c],
             device_id=(g, f, sibling), device_id_type=MESH)
 
-    def part2(s, u, k):
-        return tp_copy(sp2.at[0, place, peer(k) // 2, :, columns(s, u)], rp2.at[k // 2, :, columns(s, u)],
+    def part2(s, c, n, k):
+        return tp_copy(sp2.at[0, place, peer(k) // 2, :, columns(s, c, n)], rp2.at[k // 2, :, columns(s, c, n)],
                        p2s.at[k // 2 - 1], p2r.at[k // 2], k)
 
-    def part3(s, u, k):
-        return pltpu.make_async_remote_copy(
-            src_ref=sp2.at[1, place, peer(k) // 2, :, columns(s, u)], dst_ref=rp2.at[k // 2, :, columns(s, u)],
+    def part3(s, c, n, k):
+        return pltpu.make_async_remote_copy(
+            src_ref=sp2.at[1, place, peer(k) // 2, :, columns(s, c, n)], dst_ref=rp2.at[k // 2, :, columns(s, c, n)],
             send_sem=p3s.at[k // 2], recv_sem=p2r.at[k // 2],
             device_id=(g, helped, peer(k)), device_id_type=MESH)
 
@@ -258,10 +256,12 @@
 
     loads = [pltpu.make_async_copy(a, b, lsem.at[4 + i])
              for i, (a, b) in enumerate(((tok_h, tok), (gains_h, gains), (scale_h, scale)))]
+    local("mi", 0).start()
+    local("mo", 1).start()
     for load in loads:
         load.start()
-    for index, w in enumerate(("mi", "mo", "up", "dn")):
-        local(w, index).start()
+    local("up", 2).start()
+    local("dn", 3).start()
 
     barrier = pltpu.get_barrier_semaphore()
 
@@ -291,34 +291,48 @@
         greeted = greeted + jnp.where(helper | end, T - 1, 0)
     pl.semaphore_wait(barrier, greeted)
 
+    local("mi", 0).wait()
     send_own("mi", 0)
+    local("mo", 1).wait()
     send_own("mo", 0)
+    local("up", 2).wait()
     send_own("up", 0)
+
+    @pl.when(~mid_plane)
+    def _():
+        for c in range(1, NU):
+            send_own("up", c)
+    send_whole("up")
     for load in loads:
         load.wait()
     g1[t] = normalize(tok[...], gains[0:1, :]).astype(jnp.bfloat16)
     gather_start(g1, sems1)
+    local("dn", 3).wait()
 
     for d in range(1, F):
-        pump("mi", d, 0)
-        pump("mo", d, 0)
+        for kind in ("near", "relay"):
+            if kind == "near" or (off and d == 1):
+                pump("mi", d, 0, kind)
+                pump("mo", d, 0, kind)
         if d < NU:
-            send_own("up", d)
-    for c in range(F, NU):
-        send_own("up", c)
-    send_whole("up")
+            @pl.when(mid_plane)
+            def _():
+                send_own("up", d)
+
+    @pl.when(mid_plane)
+    def _():
+        for c in range(F, NU):
+            send_own("up", c)
 
     for c in range(NU // 2):
         pump("up", 1, c)
 
     y_wait_all("mi")
-    local("mi", 0).wait()
     gather_finish(g1, sems1)
     mixed_in = jnp.dot(g1[...].reshape(T * R, D), mi[...],
                        preferred_element_type=jnp.float32).astype(jnp.bfloat16)
     scaled = (pooling(mixed_in, t * PWt, PWt * T // GROUPS) * scale[...]).astype(jnp.bfloat16)
     y_wait_all("mo")
-    local("mo", 1).wait()
     for j in range(4):
         cols = pl.ds(j * step, step)
         value = jnp.dot(scaled, mo[:, cols], preferred_element_type=jnp.float32
@@ -401,8 +415,6 @@
 
     up_acts = {2: [("near", 1, 0)], 3: [("near", 1, 1), ("relay", 1, 0), ("near", 1, 2)], 5: [("relay", 1, 1)],
                6: [("near", 1, 3)], 7: [("relay", 1, 2)]}
-    dn_acts = {3: [("relay", 1, 3), ("near", 2, 0)], 5: [("near", 2, 1)], 7: [("near", 2, 2), ("pass", 0, 0)],
-               8: [("near", 2, 3)]}
 
     def scheduled(acts, n):
         for index, todo in acts.items():
@@ -445,48 +457,106 @@
             pump("dn", 1, jnp.where(i == 0, c - half_u, half_d))
         return 0
 
-    local("up", 2).wait()
-    local("dn", 3).wait()
-
-    def dn_compute(s, u):
-        @pl.when(s != f)
-        def _():
-            for c in range(UD):
-                if tuned and c == UD - 1:
-                    @pl.when(~(helper & (s == helped) & (u == NB - 1)))
-                    def _():
-                        y_wait("dn", s, u * UD + c)
-                else:
-                    y_wait("dn", s, u * UD + c)
-        cols = columns(s, u)
-
-        def project(i):
-            value = jnp.dot(hid[i], dn[:, cols], preferred_element_type=jnp.float32
-                            ).astype(jnp.bfloat16).reshape(half_t, 2, R, cw)
-            for q in range(2):
-                sp2[i, q, :, :, cols] = value[:, q]
-            swap2(i, s, u).start()
+    def project(i, s, first, n):
+        cols = columns(s, first, n)
+        value = jnp.dot(hid[i], dn[:, cols], preferred_element_type=jnp.float32
+                        ).astype(jnp.bfloat16).reshape(half_t, 2, R, n * cd)
+        for q in range(2):
+            sp2[i, q, :, :, cols] = value[:, q]
+        swap2(i, s, first, n).start()
+
+    def finish(i, s, first, n):
+        cols = columns(s, first, n)
+        swap2(i, s, first, n).wait_recv()
+        sp2[i, place, :, :, cols] = merge(sp2[i, place, :, :, cols], rq2[i, :, :, cols])
+
+        @pl.when(i == 0)
+        def _():
+            for k in range(2, T, 2):
+                part2(s, first, n, k).start()
         if off:
-            @pl.when(helper)
-            def _():
-                project(1)
-        project(0)
-
-    def dn_merge(s, u):
-        cols = columns(s, u)
-
-        def finish(i):
-            swap2(i, s, u).wait_recv()
-            sp2[i, place, :, :, cols] = merge(sp2[i, place, :, :, cols], rq2[i, :, :, cols])
-        if off:
-            @pl.when(helper)
-            def _():
-                finish(1)
+            @pl.when(i == 1)
+            def _():
                 for k in range(0, T, 2):
-                    part3(s, u, k).start()
-        finish(0)
-        for k in range(2, T, 2):
-            part2(s, u, k).start()
+                    part3(s, first, n, k).start()
+
+    OWN, NEAR, HELPED, FAR = range(4)
+    codes, before = [], {}
+
+    def queue(kind, who, c, n, rows=(1, 0), wait=True):
+        for i in rows:
+            fresh = kind == 0 and wait and who != OWN and i == rows[0]
+            codes.append(kind + 2 * (n - 1) + 4 * i + 8 * fresh + 16 * who + 64 * c)
+
+    def also(*todo):
+        before.setdefault(len(codes), []).extend(todo)
+
+    if tuned:
+        queue(0, OWN, 0, 2)
+        queue(0, OWN, 2, 2)
+        queue(1, OWN, 0, 2)
+        also(("relay", 1, 3), ("near", 2, 0))
+        queue(1, OWN, 2, 2)
+        queue(0, NEAR, 0, 2)
+        also(("near", 2, 1))
+        queue(1, NEAR, 0, 2)
+        queue(0, NEAR, 2, 2)
+        also(("pass", 0, 0))
+        queue(1, NEAR, 2, 2)
+        also(("near", 2, 2))
+        queue(0, HELPED, 2, 2)
+        queue(0, FAR, 0, 1)
+        queue(1, HELPED, 2, 2)
+        queue(1, FAR, 0, 1)
+        queue(0, FAR, 1, 1, (1,))
+        also(("near", 2, 3))
+        queue(0, HELPED, 0, 1, (1,))
+        queue(0, FAR, 1, 1, (0,), False)
+        queue(1, FAR, 1, 1, (1,))
+        queue(0, HELPED, 0, 1, (0,), False)
+        queue(1, HELPED, 0, 1, (1,))
+        queue(1, FAR, 1, 1, (0,))
+        queue(0, FAR, 2, 1, (1,))
+        queue(1, HELPED, 0, 1, (0,))
+        queue(0, FAR, 3, 1, (1,))
+        queue(0, HELPED, 1, 1, (1,))
+        queue(1, FAR, 2, 1, (1,))
+        queue(0, FAR, 2, 1, (0,), False)
+        queue(1, FAR, 3, 1, (1,))
+        queue(1, HELPED, 1, 1, (1,))
+        queue(0, FAR, 3, 1, (0,), False)
+        queue(0, HELPED, 1, 1, (0,), False)
+        queue(1, FAR, 2, 1, (0,))
+        queue(1, FAR, 3, 1, (0,))
+        queue(1, HELPED, 1, 1, (0,))
+
+    def choose(n, values):
+        out = jnp.int32(values[0])
+        for index, value in enumerate(values[1:]):
+            out = jnp.where(n == index + 1, value, out)
+        return out
+
+    def dn_op(n, _):
+        scheduled(before, n)
+        code = choose(n, codes)
+        kind, size, i = lax.rem(code, 2), lax.rem(code // 2, 2) + 1, lax.rem(code // 4, 2)
+        fresh, who, first = lax.rem(code // 8, 2), lax.rem(code // 16, 4), code // 64
+        s = jnp.where(who == OWN, f, jnp.where(who == NEAR, F - 1 - f, jnp.where(who == HELPED, helped, F - 1 - helped)))
+        for c in range(2):
+            passed = (who == HELPED) & (first + c == ND - 1)
+
+            @pl.when((fresh == 1) & (c < size) & ~passed)
+            def _():
+                y_wait("dn", s, first + c)
+        for width in (1, 2):
+            @pl.when((kind == 0) & (size == width))
+            def _():
+                project(i, s, first, width)
+
+            @pl.when((kind == 1) & (size == width))
+            def _():
+                finish(i, s, first, width)
+        return 0
 
     slots = (far + 1) * NB
 
@@ -494,25 +564,30 @@
         def one(now, _):
             m = n - 1 + now
             slot, q = m // 2, lax.rem(m, 2)
-            d, u = slot // NB, lax.rem(slot, NB)
+            d, first = slot // NB, lax.rem(slot, NB) * UD
             last = helper & (d == far)
             s = jnp.where(q == 0, f - d, f + d)
             s = jnp.where(last, jnp.where(q == 0, F - 1 - helped, helped), s)
             wanted = ((m >= 0) & (slot < slots) & (s >= 0) & (s < F) & ((q == 0) | (d > 0))
                       & (last | ~(helper & (s == helped))))
 
-            @pl.when(wanted & (now == 0))
-            def _():
-                dn_merge(s, u)
-
-            @pl.when(wanted & (now == 1))
-            def _():
-                dn_compute(s, u)
+            @pl.when(wanted & (now == 1) & (s != f))
+            def _():
+                for c in range(UD):
+                    y_wait("dn", s, first + c)
+
+            def rows(i, _):
+                @pl.when(wanted & (now == 0))
+                def _():
+                    finish(i, s, first, UD)
+
+                @pl.when(wanted & (now == 1))
+                def _():
+                    project(i, s, first, UD)
+                return 0
+            lax.fori_loop(0, jnp.where(helper, 2, 1), rows, 0)
             return 0
         lax.fori_loop(0, 2, one, 0)
-        if tuned:
-            scheduled(dn_acts, n)
-            return 0
         slot = n // 2
 
         @pl.when(n == 2 * NB - 1)
@@ -530,7 +605,10 @@
     def _():
         gather_finish(own_rows, sems2)
         lax.fori_loop(0, (2 if off else 1) * NU, up_step, 0)
-        lax.fori_loop(0, 2 * slots + 1, dn_step, 0)
+        if tuned:
+            lax.fori_loop(0, len(codes), dn_op, 0)
+        else:
+            lax.fori_loop(0, 2 * slots + 1, dn_step, 0)
 
     def landed(k):
         return tp_copy(rp2.at[k // 2], rp2.at[k // 2], p2s.at[0], p2r.at[k // 2], 2)
@@ -652,7 +730,7 @@
             dma((G - 1, 2, F)), dma((G - 1, F, NP)),
             dma((3,)), dma((T,)), dma((T,)), dma((T,)),
             dma((1,)), dma((1,)),
-            dma((1,)), dma((4,)), dma((2,)), dma((2, F, ND if ND % 2 else ND // 2)),
+            dma((1,)), dma((4,)), dma((2,)), dma((2, F, ND)),
             dma((H - 1,)), dma((H - 1,)),
             dma((H - 1,)), dma((H,)), dma((H,)),
         ],

time: 127 us -> 125 us (0.984)
  Pallas kernels: 126 us -> 124 us
    pallas_call x1, Pallas kernels: 126 us -> 124 us  [local_layer(): pl.pallas_call(functools.partial(kernel, dims), out_shape=pltpu.VMEM((R,...]
where the time goes in v4:
time: 125 us
  Pallas kernels  124 us (99%)
    pallas_call x1, Pallas kernels, local_layer(): pl.pallas_call(functools.partial(kernel, dims), out_shape=pltpu.VMEM((R,...  124 us

profile of v4, /device:TPU:0, one launch (start us, length us, event | category | flops | bytes accessed | tf_op | source)
XLA Modules:
  0.0 124.9 jit_solution(16274902698105551281)
XLA Ops:
  0.0 124.1 %shard_map.73 = bf16[128,2048]{1,0:T(8,128)(2,1)S(1)} custom-call(bf16[128,2048]{1,0:T(8,128)(2,1)} %tok_h.1, f32[4,2048]{1,0:T(4,128)} %gains_h.1, f32[1,256]{1,0:T(1,128)} %bitcast.1, bf16[512,256]{1,0:T(8,128)(2,1)} %mi_h.1, bf16[256,512]{1,0:T(8,128)(2,1)} %mo_h.1, bf16[512,2048]{1,0:T(8,128)(2,1)} %up_h.1, bf16[2048,512]{1,0:T(8,128)(2,1)} %dn_h.1), custom_call_target="tpu_custom_call" | custom-call | tf_op jit(solution)/shard_map/pallas_call | solution.py:715
  124.1 0.8 copy.9

commit v5 on v4

--- a/solution.py
+++ b/solution.py
@@ -66,6 +66,9 @@
     kinds = {"mi": 0, "mo": 0, "up": 1, "dn": 1}
     bufs = {"mi": (mi_h, mi), "mo": (mo_h, mo), "up": (up_h, up), "dn": (dn_h, dn)}
 
+    def slot_of(s, where):
+        return s - jnp.where(s > where, 1, 0)
+
     def mult(value, by):
         return pl.multiple_of(value, by)
 
@@ -87,7 +90,7 @@
         target = f + 1 if to_right else f - 1
         side = 0 if to_right else 1
         return pltpu.make_async_remote_copy(
-            src_ref=view(w, s, c, g), dst_ref=view(w, s, c, g), send_sem=zs.at[side, kinds[w], s], recv_sem=zr.at[s, p],
+            src_ref=view(w, s, c, g), dst_ref=view(w, s, c, g), send_sem=zs.at[side, kinds[w], s], recv_sem=zr.at[s - side, p],
             device_id=(g, target, t), device_id_type=MESH)
 
     def y_copy(w, s, c, k, half=None):
@@ -95,7 +98,7 @@
         half = g if half is None else half
         return pltpu.make_async_remote_copy(
             src_ref=view(w, s, c, half), dst_ref=view(w, s, c, half),
-            send_sem=ys.at[k - 1, kinds[w], s], recv_sem=yr.at[k - 1, s, p],
+            send_sem=ys.at[k - 1, kinds[w], s], recv_sem=yr.at[k - 1, slot_of(s, f), p],
             device_id=(lax.rem(g + k, G), f, t), device_id_type=MESH)
 
     def send_own(w, c):
@@ -112,7 +115,7 @@
         half = lax.rem(g - k + G, G)
         return pltpu.make_async_remote_copy(
             src_ref=view(w, f, c, half), dst_ref=view(w, f, c, half),
-            send_sem=ys.at[k - 1, kinds[w], f], recv_sem=yr.at[k - 1, f, p],
+            send_sem=ys.at[k - 1, kinds[w], f], recv_sem=yr.at[k - 1, slot_of(f, inner), p],
             device_id=(g, inner, t), device_id_type=MESH)
 
     def send_whole(w):
@@ -132,7 +135,7 @@
         p = pieces["dn"][0] + ND - 1
         block = view("dn", helped, ND - 1, half)
         return pltpu.make_async_remote_copy(
-            src_ref=block, dst_ref=block, send_sem=ys.at[k - 1, 1, helped], recv_sem=yr.at[k - 1, helped, p],
+            src_ref=block, dst_ref=block, send_sem=ys.at[k - 1, 1, helped], recv_sem=yr.at[k - 1, slot_of(helped, F - 1 - f), p],
             device_id=(g, F - 1 - f, t), device_id_type=MESH)
 
     def pump(w, d, c, kind=None):
@@ -278,17 +281,6 @@
     for k in range(1, T):
         pl.semaphore_signal(barrier, inc=1, device_id=(g, f, peer(k)), device_id_type=MESH)
     greeted = jnp.where(f + 1 < F, 1, 0) + jnp.where(f > 0, 1, 0) + (G - 1 + T - 1)
-    if off:
-        @pl.when(helper)
-        def _():
-            for k in range(1, T):
-                pl.semaphore_signal(barrier, inc=1, device_id=(g, helped, peer(k)), device_id_type=MESH)
-
-        @pl.when(end)
-        def _():
-            for k in range(1, T):
-                pl.semaphore_signal(barrier, inc=1, device_id=(g, inner, peer(k)), device_id_type=MESH)
-        greeted = greeted + jnp.where(helper | end, T - 1, 0)
     pl.semaphore_wait(barrier, greeted)
 
     local("mi", 0).wait()
@@ -480,13 +472,26 @@
                 for k in range(0, T, 2):
                     part3(s, first, n, k).start()
 
+    def project_pair(i, left, right):
+        cols = [columns(s, c, 1) for s, c in (left, right)]
+        both = jnp.concatenate([dn[:, col] for col in cols], axis=1)
+        value = jnp.dot(hid[i], both, preferred_element_type=jnp.float32).astype(jnp.bfloat16)
+        for j, (s, c) in enumerate((left, right)):
+            part = value[:, j * cd:(j + 1) * cd].reshape(half_t, 2, R, cd)
+            for q in range(2):
+                sp2[i, q, :, :, cols[j]] = part[:, q]
+            swap2(i, s, c, 1).start()
+
     OWN, NEAR, HELPED, FAR = range(4)
-    codes, before = [], {}
+    codes, before, PAIR = [], {}, 64 * ND
 
     def queue(kind, who, c, n, rows=(1, 0), wait=True):
         for i in rows:
             fresh = kind == 0 and wait and who != OWN and i == rows[0]
             codes.append(kind + 2 * (n - 1) + 4 * i + 8 * fresh + 16 * who + 64 * c)
+
+    def queue_pair(i, fresh):
+        codes.append(4 * i + 8 * fresh + 16 * FAR + 64 * (ND - 1) + PAIR)
 
     def also(*todo):
         before.setdefault(len(codes), []).extend(todo)
@@ -518,14 +523,12 @@
         queue(1, FAR, 1, 1, (0,))
         queue(0, FAR, 2, 1, (1,))
         queue(1, HELPED, 0, 1, (0,))
-        queue(0, FAR, 3, 1, (1,))
-        queue(0, HELPED, 1, 1, (1,))
+        queue_pair(1, True)
         queue(1, FAR, 2, 1, (1,))
         queue(0, FAR, 2, 1, (0,), False)
         queue(1, FAR, 3, 1, (1,))
         queue(1, HELPED, 1, 1, (1,))
-        queue(0, FAR, 3, 1, (0,), False)
-        queue(0, HELPED, 1, 1, (0,), False)
+        queue_pair(0, False)
         queue(1, FAR, 2, 1, (0,))
         queue(1, FAR, 3, 1, (0,))
         queue(1, HELPED, 1, 1, (0,))
@@ -539,6 +542,8 @@
     def dn_op(n, _):
         scheduled(before, n)
         code = choose(n, codes)
+        pair = code >= PAIR
+        code = lax.rem(code, PAIR)
         kind, size, i = lax.rem(code, 2), lax.rem(code // 2, 2) + 1, lax.rem(code // 4, 2)
         fresh, who, first = lax.rem(code // 8, 2), lax.rem(code // 16, 4), code // 64
         s = jnp.where(who == OWN, f, jnp.where(who == NEAR, F - 1 - f, jnp.where(who == HELPED, helped, F - 1 - helped)))
@@ -548,8 +553,16 @@
             @pl.when((fresh == 1) & (c < size) & ~passed)
             def _():
                 y_wait("dn", s, first + c)
+
+        @pl.when((fresh == 1) & pair)
+        def _():
+            y_wait("dn", helped, 1)
+
+        @pl.when(pair)
+        def _():
+            project_pair(i, (s, first), (helped, 1))
         for width in (1, 2):
-            @pl.when((kind == 0) & (size == width))
+            @pl.when((kind == 0) & (size == width) & ~pair)
             def _():
                 project(i, s, first, width)
 
@@ -726,8 +739,8 @@
             pltpu.VMEM((2, H, R, D), bf), pltpu.VMEM((H, R, D), bf), pltpu.VMEM((H - 1, R, D), bf),
             pltpu.VMEM((2, 2, H, R, D), bf), pltpu.VMEM((2, H, R, D), bf), pltpu.VMEM((H, R, D), bf),
             pltpu.VMEM((R, D), bf),
-            dma((7,)), dma((2, 2, F)), dma((F, NP)),
-            dma((G - 1, 2, F)), dma((G - 1, F, NP)),
+            dma((7,)), dma((2, 2, F)), dma((F - 1, NP)),
+            dma((G - 1, 2, F)), dma((G - 1, F - 1, NP)),
             dma((3,)), dma((T,)), dma((T,)), dma((T,)),
             dma((1,)), dma((1,)),
             dma((1,)), dma((4,)), dma((2,)), dma((2, F, ND)),

time: 125 us -> 124 us (level)
  no operation moved by 1% of the time
where the time goes in v5:
time: 124 us
  Pallas kernels  123 us (99%)
    pallas_call x1, Pallas kernels, local_layer(): pl.pallas_call(functools.partial(kernel, dims), out_shape=pltpu.VMEM((R,...  123 us

profile of v5, /device:TPU:0, one launch (start us, length us, event | category | flops | bytes accessed | tf_op | source)
XLA Modules:
  0.0 124.1 jit_solution(13428708844897301503)
XLA Ops:
  0.0 123.3 %shard_map.73 = bf16[128,2048]{1,0:T(8,128)(2,1)S(1)} custom-call(bf16[128,2048]{1,0:T(8,128)(2,1)} %tok_h.1, f32[4,2048]{1,0:T(4,128)} %gains_h.1, f32[1,256]{1,0:T(1,128)} %bitcast.1, bf16[512,256]{1,0:T(8,128)(2,1)} %mi_h.1, bf16[256,512]{1,0:T(8,128)(2,1)} %mo_h.1, bf16[512,2048]{1,0:T(8,128)(2,1)} %up_h.1, bf16[2048,512]{1,0:T(8,128)(2,1)} %dn_h.1), custom_call_target="tpu_custom_call" | custom-call | tf_op jit(solution)/shard_map/pallas_call | solution.py:728
  123.3 0.8 copy.9

commit v6 on v5

--- a/solution.py
+++ b/solution.py
@@ -36,7 +36,7 @@
            tok, gains, scale, mi, mo, up, dn, g1, g2, hid, sp1, rq1, rp1, sp2, rq2, rp2, mid,
            lsem, zs, zr, ys, yr, gs, g1r, g2r, g3r, es, er,
            w1s, w1r, w2s, w2r, p1s, p1r, p2s, p2r, p3s):
-    G, F, T, R, D, K, PWt, Ht, NU, ND = dims
+    G, F, T, R, D, K, PWt, Ht, NU, ND, NP = dims
     g, f, t = lax.axis_index("grp"), lax.axis_index("fs"), lax.axis_index("tp")
     cu, cd = Ht // NU, K // ND
     UD = 1 if ND % 2 else 2
@@ -62,12 +62,26 @@
 
     def shared(w, s):
         return True if w in ("mi", "mo") or not off else ~(helper & (s == helped))
-    pieces = {"mi": (0, 1), "mo": (1, 1), "up": (2, NU), "dn": (2 + NU, ND)}
+    NM = 1
+    pieces = {"mi": (0, NM), "mo": (NM, 1), "up": (NM + 1, NU), "dn": (NM + 1 + NU, ND)}
     kinds = {"mi": 0, "mo": 0, "up": 1, "dn": 1}
     bufs = {"mi": (mi_h, mi), "mo": (mo_h, mo), "up": (up_h, up), "dn": (dn_h, dn)}
 
     def slot_of(s, where):
         return s - jnp.where(s > where, 1, 0)
+
+    def zsem(side, kind, s):
+        return zs.at[side, 0, 0] if tuned else zs.at[side, kind, s]
+
+    def ysem(k, kind, s):
+        return ys.at[k - 1, 0, 0] if tuned else ys.at[k - 1, kind, s]
+
+    def yrsem(k, w, s, c, where):
+        slot = slot_of(s, where)
+        if not tuned:
+            return yr.at[k - 1, slot * NP + pieces[w][0] + c]
+        base = {"mi": 0, "mo": 1, "up": 2, "dn": 2 + NU + slot * ND}[w]
+        return yr.at[k - 1, base + c]
 
     def mult(value, by):
         return pl.multiple_of(value, by)
@@ -75,7 +89,8 @@
     def span(w, s, c, half):
         base = s * K
         if w == "mi":
-            return pl.ds(mult(base + half * (K // G), K // G), K // G), pl.ds(0, PWt)
+            size = K // G // NM
+            return pl.ds(mult(base + (half * NM + c) * size, size), size), pl.ds(0, PWt)
         if w == "mo":
             return pl.ds(mult(half * (PWt // G), PWt // G), PWt // G), pl.ds(mult(base, 128), K)
         if w == "up":
@@ -90,15 +105,14 @@
         target = f + 1 if to_right else f - 1
         side = 0 if to_right else 1
         return pltpu.make_async_remote_copy(
-            src_ref=view(w, s, c, g), dst_ref=view(w, s, c, g), send_sem=zs.at[side, kinds[w], s], recv_sem=zr.at[s - side, p],
+            src_ref=view(w, s, c, g), dst_ref=view(w, s, c, g), send_sem=zsem(side, kinds[w], s), recv_sem=zr.at[s - side, p],
             device_id=(g, target, t), device_id_type=MESH)
 
     def y_copy(w, s, c, k, half=None):
-        p = pieces[w][0] + c
         half = g if half is None else half
         return pltpu.make_async_remote_copy(
             src_ref=view(w, s, c, half), dst_ref=view(w, s, c, half),
-            send_sem=ys.at[k - 1, kinds[w], s], recv_sem=yr.at[k - 1, slot_of(s, f), p],
+            send_sem=ysem(k, kinds[w], s), recv_sem=yrsem(k, w, s, c, f),
             device_id=(lax.rem(g + k, G), f, t), device_id_type=MESH)
 
     def send_own(w, c):
@@ -111,11 +125,10 @@
             z_copy(w, f, c, False).start()
 
     def whole_copy(w, c, k):
-        p = pieces[w][0] + c
         half = lax.rem(g - k + G, G)
         return pltpu.make_async_remote_copy(
             src_ref=view(w, f, c, half), dst_ref=view(w, f, c, half),
-            send_sem=ys.at[k - 1, kinds[w], f], recv_sem=yr.at[k - 1, slot_of(f, inner), p],
+            send_sem=ysem(k, kinds[w], f), recv_sem=yrsem(k, w, f, c, inner),
             device_id=(g, inner, t), device_id_type=MESH)
 
     def send_whole(w):
@@ -132,10 +145,9 @@
 
     def pass_on(k):
         half = lax.rem(g - k + G, G)
-        p = pieces["dn"][0] + ND - 1
         block = view("dn", helped, ND - 1, half)
         return pltpu.make_async_remote_copy(
-            src_ref=block, dst_ref=block, send_sem=ys.at[k - 1, 1, helped], recv_sem=yr.at[k - 1, slot_of(helped, F - 1 - f), p],
+            src_ref=block, dst_ref=block, send_sem=ysem(k, 1, helped), recv_sem=yrsem(k, "dn", helped, ND - 1, F - 1 - f),
             device_id=(g, F - 1 - f, t), device_id_type=MESH)
 
     def pump(w, d, c, kind=None):
@@ -169,7 +181,23 @@
         for k in range(1, G):
             y_copy(w, s, c, k, lax.rem(g - k + G, G)).wait_recv()
 
+    def y_wait_rows(w, c):
+        size, cols = (F - 1) * (K // G), pl.ds(0, PWt)
+        if w == "mo":
+            size, cols = PWt // G, pl.ds(0, (F - 1) * K)
+        if w == "up":
+            cols = pl.ds(mult(c * cu, cu), cu)
+        rows = bufs[w][1].at[pl.ds(0, size), cols]
+        for k in range(1, G):
+            pltpu.make_async_remote_copy(
+                src_ref=rows, dst_ref=rows, send_sem=ysem(k, 0, 0), recv_sem=yrsem(k, w, 0, c, f),
+                device_id=(lax.rem(g + k, G), f, t), device_id_type=MESH).wait_recv()
+
     def y_wait_all(w):
+        if tuned:
+            y_wait_rows(w, 0)
+            return
+
         def body(i, _):
             s, c = i // pieces[w][1], lax.rem(i, pieces[w][1])
 
@@ -238,10 +266,16 @@
     def columns(s, c, n):
         return pl.ds(mult(s * K + c * cd, cd), n * cd)
 
+    def swap_index(s, c):
+        if not tuned:
+            return s * ND + c
+        base = jnp.where(s == f, 2 * ND - 1, 2 * ND + 1) + c // 2
+        return jnp.where(s == helped, c, jnp.where(s == F - 1 - helped, ND - 1 + c, base))
+
     def swap2(i, s, c, n):
         return pltpu.make_async_remote_copy(
             src_ref=sp2.at[i, 1 - place, :, :, columns(s, c, n)], dst_ref=rq2.at[i, :, :, columns(s, c, n)],
-            send_sem=w2s.at[i], recv_sem=w2r.at[i, s, c],
+            send_sem=w2s.at[i], recv_sem=w2r.at[i, swap_index(s, c)],
             device_id=(g, f, sibling), device_id_type=MESH)
 
     def part2(s, c, n, k):
@@ -284,7 +318,8 @@
     pl.semaphore_wait(barrier, greeted)
 
     local("mi", 0).wait()
-    send_own("mi", 0)
+    for c in range(NM):
+        send_own("mi", c)
     local("mo", 1).wait()
     send_own("mo", 0)
     local("up", 2).wait()
@@ -304,12 +339,15 @@
     for d in range(1, F):
         for kind in ("near", "relay"):
             if kind == "near" or (off and d == 1):
-                pump("mi", d, 0, kind)
+                for c in range(NM):
+                    pump("mi", d, c, kind)
                 pump("mo", d, 0, kind)
         if d < NU:
             @pl.when(mid_plane)
             def _():
                 send_own("up", d)
+        if tuned and d == 1:
+            pump("up", 1, 0, "near")
 
     @pl.when(mid_plane)
     def _():
@@ -317,7 +355,7 @@
             send_own("up", c)
 
     for c in range(NU // 2):
-        pump("up", 1, c)
+        pump("up", 1, c, "relay" if tuned and c == 0 else None)
 
     y_wait_all("mi")
     gather_finish(g1, sems1)
@@ -325,6 +363,8 @@
                        preferred_element_type=jnp.float32).astype(jnp.bfloat16)
     scaled = (pooling(mixed_in, t * PWt, PWt * T // GROUPS) * scale[...]).astype(jnp.bfloat16)
     y_wait_all("mo")
+    if tuned:
+        pump("up", 1, NU // 2)
     for j in range(4):
         cols = pl.ds(j * step, step)
         value = jnp.dot(scaled, mo[:, cols], preferred_element_type=jnp.float32
@@ -345,7 +385,9 @@
             return 0
         lax.fori_loop(start, pieces[w][1], body, 0)
 
-    pump_all("up", 1, NU // 2)
+    pump_all("up", 1, NU // 2 + 1 if tuned else NU // 2)
+    if tuned:
+        pump("up", far, 0)
     early = far <= 2
 
     @pl.when(mid_plane & early)
@@ -381,7 +423,7 @@
             send_own("dn", c)
     send_whole("dn")
     if far > 1:
-        pump_all("up", far)
+        pump_all("up", far, 1 if tuned else 0)
 
     def up_project(i, c):
         cols = pl.ds(mult(c * cu, cu), cu)
@@ -419,6 +461,10 @@
 
         @pl.when(i == 0)
         def _():
+            if tuned:
+                y_wait_rows("up", c)
+                return
+
             def landed_rows(s, _):
                 @pl.when(s != f)
                 def _():
@@ -469,8 +515,8 @@
         if off:
             @pl.when(i == 1)
             def _():
-                for k in range(0, T, 2):
-                    part3(s, first, n, k).start()
+                for chip in range(half_t):
+                    part3(s, first, n, lax.rem(2 * chip + place - t + T, T)).start()
 
     def project_pair(i, left, right):
         cols = [columns(s, c, 1) for s, c in (left, right)]
@@ -500,7 +546,7 @@
         queue(0, OWN, 0, 2)
         queue(0, OWN, 2, 2)
         queue(1, OWN, 0, 2)
-        also(("relay", 1, 3), ("near", 2, 0))
+        also(("near", 2, 0), ("relay", 1, 3))
         queue(1, OWN, 2, 2)
         queue(0, NEAR, 0, 2)
         also(("near", 2, 1))
@@ -521,17 +567,31 @@
         queue(0, HELPED, 0, 1, (0,), False)
         queue(1, HELPED, 0, 1, (1,))
         queue(1, FAR, 1, 1, (0,))
-        queue(0, FAR, 2, 1, (1,))
         queue(1, HELPED, 0, 1, (0,))
-        queue_pair(1, True)
-        queue(1, FAR, 2, 1, (1,))
-        queue(0, FAR, 2, 1, (0,), False)
-        queue(1, FAR, 3, 1, (1,))
-        queue(1, HELPED, 1, 1, (1,))
-        queue_pair(0, False)
-        queue(1, FAR, 2, 1, (0,))
-        queue(1, FAR, 3, 1, (0,))
-        queue(1, HELPED, 1, 1, (0,))
+        tails = []
+        split = len(codes)
+        for second in (False, True):
+            if second:
+                queue_pair(1, True)
+                queue(0, FAR, 2, 1, (1,))
+                queue_pair(0, False)
+                queue(0, FAR, 2, 1, (0,), False)
+                queue(1, FAR, 3, 1, (1,))
+                queue(1, HELPED, 1, 1, (1,))
+                queue(1, FAR, 2, 1, (1,))
+            else:
+                queue_pair(1, True)
+                queue(0, FAR, 2, 1, (1,))
+                queue(1, FAR, 3, 1, (1,))
+                queue(1, HELPED, 1, 1, (1,))
+                queue_pair(0, False)
+                queue(1, FAR, 2, 1, (1,))
+                queue(0, FAR, 2, 1, (0,), False)
+            queue(1, FAR, 3, 1, (0,))
+            queue(1, HELPED, 1, 1, (0,))
+            queue(1, FAR, 2, 1, (0,))
+            tails.append(codes[split:])
+            del codes[split:]
 
     def choose(n, values):
         out = jnp.int32(values[0])
@@ -541,14 +601,14 @@
 
     def dn_op(n, _):
         scheduled(before, n)
-        code = choose(n, codes)
+        code = jnp.where(place == 0, choose(n, codes + tails[0]), choose(n, codes + tails[1]))
         pair = code >= PAIR
         code = lax.rem(code, PAIR)
         kind, size, i = lax.rem(code, 2), lax.rem(code // 2, 2) + 1, lax.rem(code // 4, 2)
         fresh, who, first = lax.rem(code // 8, 2), lax.rem(code // 16, 4), code // 64
         s = jnp.where(who == OWN, f, jnp.where(who == NEAR, F - 1 - f, jnp.where(who == HELPED, helped, F - 1 - helped)))
         for c in range(2):
-            passed = (who == HELPED) & (first + c == ND - 1)
+            passed = ((who == HELPED) & (first + c == ND - 1)) | pair
 
             @pl.when((fresh == 1) & (c < size) & ~passed)
             def _():
@@ -557,6 +617,7 @@
         @pl.when((fresh == 1) & pair)
         def _():
             y_wait("dn", helped, 1)
+            y_wait("dn", s, ND - 1)
 
         @pl.when(pair)
         def _():
@@ -619,7 +680,7 @@
         gather_finish(own_rows, sems2)
         lax.fori_loop(0, (2 if off else 1) * NU, up_step, 0)
         if tuned:
-            lax.fori_loop(0, len(codes), dn_op, 0)
+            lax.fori_loop(0, len(codes + tails[0]), dn_op, 0)
         else:
             lax.fori_loop(0, 2 * slots + 1, dn_step, 0)
 
@@ -653,7 +714,28 @@
             src_ref=buf, dst_ref=buf, send_sem=sem, recv_sem=w1r.at[0],
             device_id=(g, f, sibling), device_id_type=MESH).wait_send()
 
-    for kind, w in ((0, "mi"), (1, "up")):
+    if tuned:
+        large = 2 * (K // G)
+        small = large * PWt // Ht
+
+        def gone(amount, sem):
+            swapped(up.at[pl.ds(0, amount[0] * small + amount[1] * large), :], sem)
+
+        for side, plans in enumerate((((0, (1, 1)), (1, (2, 2)), (2, (3, 0))), ((3, (1, 1)), (2, (2, 2)), (1, (3, 0))))):
+            for place_f, amount in plans:
+                @pl.when(f == place_f)
+                def _():
+                    gone(amount, zsem(side, 0, 0))
+        for k in range(1, G):
+            @pl.when(mid_plane)
+            def _():
+                gone((3, 2), ysem(k, 0, 0))
+
+            @pl.when(end)
+            def _():
+                gone((3, 1), ysem(k, 0, 0))
+
+    for kind, w in () if tuned else ((0, "mi"), (1, "up")):
         def drain(s, _):
             moved = True if kind == 0 else (mid_plane | (s == f))
 
@@ -665,23 +747,10 @@
             def _():
                 sent(kind, zs.at[1, kind, s])
 
-            gone = (s != f) & moved & shared(w, s)
-            ends = (s == 0) | (s == F - 1) if tuned and kind == 1 else s < 0
-
-            @pl.when(gone & ~ends)
+            @pl.when((s != f) & moved & shared(w, s))
             def _():
                 for k in range(1, G):
                     sent(kind, ys.at[k - 1, kind, s])
-            if tuned and kind == 1:
-                @pl.when(gone & ends)
-                def _():
-                    for k in range(1, G):
-                        swapped(up.at[pl.ds(0, 2 * (K // G) - cd // G), :], ys.at[k - 1, kind, s])
-
-                @pl.when(helper & (s == helped))
-                def _():
-                    for k in range(1, G):
-                        swapped(view("dn", 0, 0, 0), ys.at[k - 1, kind, s])
             if off and kind == 1:
                 @pl.when((s == f) & end)
                 def _():
@@ -720,8 +789,10 @@
     Ht = up_w.shape[1]
     NU = max(1, min(4, Ht // 256))
     ND = max(1, min(4, K // 128))
-    dims = (G, F, T, R, D, K, PWt, Ht, NU, ND)
     NP = 2 + NU + ND
+    dims = (G, F, T, R, D, K, PWt, Ht, NU, ND, NP)
+    tuned = F == 4 and NU == 4 and ND == 4
+    kinds, arrivals = (1, 1) if tuned else (2, F), 2 + NU + (F - 1) * ND if tuned else (F - 1) * NP
     H = T // 2
     vmem, hbm = pl.BlockSpec(memory_space=pltpu.VMEM), pl.BlockSpec(memory_space=pl.ANY)
     bf, dma = jnp.bfloat16, pltpu.SemaphoreType.DMA
@@ -739,11 +810,11 @@
             pltpu.VMEM((2, H, R, D), bf), pltpu.VMEM((H, R, D), bf), pltpu.VMEM((H - 1, R, D), bf),
             pltpu.VMEM((2, 2, H, R, D), bf), pltpu.VMEM((2, H, R, D), bf), pltpu.VMEM((H, R, D), bf),
             pltpu.VMEM((R, D), bf),
-            dma((7,)), dma((2, 2, F)), dma((F - 1, NP)),
-            dma((G - 1, 2, F)), dma((G - 1, F - 1, NP)),
+            dma((7,)), dma((2,) + kinds), dma((F - 1, NP)),
+            dma((G - 1,) + kinds), dma((G - 1, arrivals)),
             dma((3,)), dma((T,)), dma((T,)), dma((T,)),
             dma((1,)), dma((1,)),
-            dma((1,)), dma((4,)), dma((2,)), dma((2, F, ND)),
+            dma((1,)), dma((4,)), dma((2,)), dma((2, 2 * ND + 3 if tuned else F * ND)),
             dma((H - 1,)), dma((H - 1,)),
             dma((H - 1,)), dma((H,)), dma((H,)),
         ],

time: 124 us -> 123 us (level)
    pallas_call x1, Pallas kernels: 123 us -> 122 us  [local_layer(): pl.pallas_call(functools.partial(kernel, dims), out_shape=pltpu.VMEM((R,...]
where the time goes in v6:
time: 123 us
  Pallas kernels  122 us (99%)
    pallas_call x1, Pallas kernels, local_layer(): pl.pallas_call(functools.partial(kernel, dims), out_shape=pltpu.VMEM((R,...  122 us

profile of v6, /device:TPU:0, one launch (start us, length us, event | category | flops | bytes accessed | tf_op | source)
XLA Modules:
  0.0 122.6 jit_solution(2807670677232391314)
XLA Ops:
  0.0 121.8 %shard_map.73 = bf16[128,2048]{1,0:T(8,128)(2,1)S(1)} custom-call(bf16[128,2048]{1,0:T(8,128)(2,1)} %tok_h.1, f32[4,2048]{1,0:T(4,128)} %gains_h.1, f32[1,256]{1,0:T(1,128)} %bitcast.1, bf16[512,256]{1,0:T(8,128)(2,1)} %mi_h.1, bf16[256,512]{1,0:T(8,128)(2,1)} %mo_h.1, bf16[512,2048]{1,0:T(8,128)(2,1)} %up_h.1, bf16[2048,512]{1,0:T(8,128)(2,1)} %dn_h.1), custom_call_target="tpu_custom_call" | custom-call | tf_op jit(solution)/shard_map/pallas_call | solution.py:799
  121.9 0.8 copy.9

commit v7 on v6

--- a/solution.py
+++ b/solution.py
@@ -567,17 +567,17 @@
         queue(0, HELPED, 0, 1, (0,), False)
         queue(1, HELPED, 0, 1, (1,))
         queue(1, FAR, 1, 1, (0,))
-        queue(1, HELPED, 0, 1, (0,))
         tails = []
         split = len(codes)
         for second in (False, True):
             if second:
                 queue_pair(1, True)
                 queue(0, FAR, 2, 1, (1,))
+                queue(1, HELPED, 0, 1, (0,))
                 queue_pair(0, False)
-                queue(0, FAR, 2, 1, (0,), False)
                 queue(1, FAR, 3, 1, (1,))
                 queue(1, HELPED, 1, 1, (1,))
+                queue(0, FAR, 2, 1, (0,), False)
                 queue(1, FAR, 2, 1, (1,))
             else:
                 queue_pair(1, True)
@@ -587,9 +587,10 @@
                 queue_pair(0, False)
                 queue(1, FAR, 2, 1, (1,))
                 queue(0, FAR, 2, 1, (0,), False)
+                queue(1, HELPED, 0, 1, (0,))
+            queue(1, FAR, 2, 1, (0,))
             queue(1, FAR, 3, 1, (0,))
             queue(1, HELPED, 1, 1, (0,))
-            queue(1, FAR, 2, 1, (0,))
             tails.append(codes[split:])
             del codes[split:]
 

time: 123 us -> 123 us (level)
  no operation moved by 1% of the time
where the time goes in v7:
time: 123 us
  Pallas kernels  122 us (99%)
    pallas_call x1, Pallas kernels, local_layer(): pl.pallas_call(functools.partial(kernel, dims), out_shape=pltpu.VMEM((R,...  122 us

profile of v7, /device:TPU:0, one launch (start us, length us, event | category | flops | bytes accessed | tf_op | source)
XLA Modules:
  0.0 123.3 jit_solution(10036667665616061618)
XLA Ops:
  0.0 122.5 %shard_map.73 = bf16[128,2048]{1,0:T(8,128)(2,1)S(1)} custom-call(bf16[128,2048]{1,0:T(8,128)(2,1)} %tok_h.1, f32[4,2048]{1,0:T(4,128)} %gains_h.1, f32[1,256]{1,0:T(1,128)} %bitcast.1, bf16[512,256]{1,0:T(8,128)(2,1)} %mi_h.1, bf16[256,512]{1,0:T(8,128)(2,1)} %mo_h.1, bf16[512,2048]{1,0:T(8,128)(2,1)} %up_h.1, bf16[2048,512]{1,0:T(8,128)(2,1)} %dn_h.1), custom_call_target="tpu_custom_call" | custom-call | tf_op jit(solution)/shard_map/pallas_call | solution.py:800
  122.5 0.8 copy.9

commit v8 on v6

--- a/solution.py
+++ b/solution.py
@@ -518,26 +518,13 @@
                 for chip in range(half_t):
                     part3(s, first, n, lax.rem(2 * chip + place - t + T, T)).start()
 
-    def project_pair(i, left, right):
-        cols = [columns(s, c, 1) for s, c in (left, right)]
-        both = jnp.concatenate([dn[:, col] for col in cols], axis=1)
-        value = jnp.dot(hid[i], both, preferred_element_type=jnp.float32).astype(jnp.bfloat16)
-        for j, (s, c) in enumerate((left, right)):
-            part = value[:, j * cd:(j + 1) * cd].reshape(half_t, 2, R, cd)
-            for q in range(2):
-                sp2[i, q, :, :, cols[j]] = part[:, q]
-            swap2(i, s, c, 1).start()
-
     OWN, NEAR, HELPED, FAR = range(4)
-    codes, before, PAIR = [], {}, 64 * ND
+    codes, before = [], {}
 
     def queue(kind, who, c, n, rows=(1, 0), wait=True):
         for i in rows:
             fresh = kind == 0 and wait and who != OWN and i == rows[0]
             codes.append(kind + 2 * (n - 1) + 4 * i + 8 * fresh + 16 * who + 64 * c)
-
-    def queue_pair(i, fresh):
-        codes.append(4 * i + 8 * fresh + 16 * FAR + 64 * (ND - 1) + PAIR)
 
     def also(*todo):
         before.setdefault(len(codes), []).extend(todo)
@@ -567,29 +554,29 @@
         queue(0, HELPED, 0, 1, (0,), False)
         queue(1, HELPED, 0, 1, (1,))
         queue(1, FAR, 1, 1, (0,))
-        queue(1, HELPED, 0, 1, (0,))
         tails = []
         split = len(codes)
         for second in (False, True):
             if second:
-                queue_pair(1, True)
-                queue(0, FAR, 2, 1, (1,))
-                queue_pair(0, False)
-                queue(0, FAR, 2, 1, (0,), False)
-                queue(1, FAR, 3, 1, (1,))
+                queue(0, HELPED, 1, 1, (1,))
+                queue(0, FAR, 2, 2, (1,))
                 queue(1, HELPED, 1, 1, (1,))
-                queue(1, FAR, 2, 1, (1,))
+                queue(0, HELPED, 1, 1, (0,), False)
+                queue(1, HELPED, 0, 1, (0,))
+                queue(1, FAR, 2, 2, (1,))
+                queue(0, FAR, 2, 2, (0,), False)
+                queue(1, HELPED, 1, 1, (0,))
+                queue(1, FAR, 2, 2, (0,))
             else:
-                queue_pair(1, True)
-                queue(0, FAR, 2, 1, (1,))
-                queue(1, FAR, 3, 1, (1,))
+                queue(0, HELPED, 1, 1, (1,))
+                queue(0, FAR, 2, 2, (1,))
                 queue(1, HELPED, 1, 1, (1,))
-                queue_pair(0, False)
-                queue(1, FAR, 2, 1, (1,))
-                queue(0, FAR, 2, 1, (0,), False)
-            queue(1, FAR, 3, 1, (0,))
-            queue(1, HELPED, 1, 1, (0,))
-            queue(1, FAR, 2, 1, (0,))
+                queue(0, HELPED, 1, 1, (0,), False)
+                queue(1, FAR, 2, 2, (1,))
+                queue(0, FAR, 2, 2, (0,), False)
+                queue(1, HELPED, 0, 1, (0,))
+                queue(1, HELPED, 1, 1, (0,))
+                queue(1, FAR, 2, 2, (0,))
             tails.append(codes[split:])
             del codes[split:]
 
@@ -602,28 +589,18 @@
     def dn_op(n, _):
         scheduled(before, n)
         code = jnp.where(place == 0, choose(n, codes + tails[0]), choose(n, codes + tails[1]))
-        pair = code >= PAIR
-        code = lax.rem(code, PAIR)
         kind, size, i = lax.rem(code, 2), lax.rem(code // 2, 2) + 1, lax.rem(code // 4, 2)
         fresh, who, first = lax.rem(code // 8, 2), lax.rem(code // 16, 4), code // 64
         s = jnp.where(who == OWN, f, jnp.where(who == NEAR, F - 1 - f, jnp.where(who == HELPED, helped, F - 1 - helped)))
         for c in range(2):
-            passed = ((who == HELPED) & (first + c == ND - 1)) | pair
+            passed = (who == HELPED) & (first + c == ND - 1)
 
             @pl.when((fresh == 1) & (c < size) & ~passed)
             def _():
                 y_wait("dn", s, first + c)
 
-        @pl.when((fresh == 1) & pair)
-        def _():
-            y_wait("dn", helped, 1)
-            y_wait("dn", s, ND - 1)
-
-        @pl.when(pair)
-        def _():
-            project_pair(i, (s, first), (helped, 1))
         for width in (1, 2):
-            @pl.when((kind == 0) & (size == width) & ~pair)
+            @pl.when((kind == 0) & (size == width))
             def _():
                 project(i, s, first, width)
 

time: 123 us -> 122 us (level)
    pallas_call x1, Pallas kernels: 122 us -> 121 us  [local_layer(): pl.pallas_call(functools.partial(kernel, dims), out_shape=pltpu.VMEM((R,...]
where the time goes in v8:
time: 122 us; the launch traced here: 121 us
  Pallas kernels  121 us (99%)
    pallas_call x1, Pallas kernels, local_layer(): pl.pallas_call(functools.partial(kernel, dims), out_shape=pltpu.VMEM((R,...  121 us

profile of v8, /device:TPU:0, one launch (start us, length us, event | category | flops | bytes accessed | tf_op | source)
XLA Modules:
  0.0 121.4 jit_solution(5244542977315887174)
XLA Ops:
  0.0 120.6 %shard_map.73 = bf16[128,2048]{1,0:T(8,128)(2,1)S(1)} custom-call(bf16[128,2048]{1,0:T(8,128)(2,1)} %tok_h.1, f32[4,2048]{1,0:T(4,128)} %gains_h.1, f32[1,256]{1,0:T(1,128)} %bitcast.1, bf16[512,256]{1,0:T(8,128)(2,1)} %mi_h.1, bf16[256,512]{1,0:T(8,128)(2,1)} %mo_h.1, bf16[512,2048]{1,0:T(8,128)(2,1)} %up_h.1, bf16[2048,512]{1,0:T(8,128)(2,1)} %dn_h.1), custom_call_target="tpu_custom_call" | custom-call | tf_op jit(solution)/shard_map/pallas_call | solution.py:776
  120.6 0.8 copy.9

commit v9 on v8

--- a/solution.py
+++ b/solution.py
@@ -562,9 +562,9 @@
                 queue(0, FAR, 2, 2, (1,))
                 queue(1, HELPED, 1, 1, (1,))
                 queue(0, HELPED, 1, 1, (0,), False)
-                queue(1, HELPED, 0, 1, (0,))
                 queue(1, FAR, 2, 2, (1,))
                 queue(0, FAR, 2, 2, (0,), False)
+                queue(1, HELPED, 0, 1, (0,))
                 queue(1, HELPED, 1, 1, (0,))
                 queue(1, FAR, 2, 2, (0,))
             else:

time: 122 us -> 122 us (level)
  no operation moved by 1% of the time
where the time goes in v9:
time: 122 us; the launch traced here: 121 us
  Pallas kernels  121 us (99%)
    pallas_call x1, Pallas kernels, local_layer(): pl.pallas_call(functools.partial(kernel, dims), out_shape=pltpu.VMEM((R,...  121 us

profile of v9, /device:TPU:0, one launch (start us, length us, event | category | flops | bytes accessed | tf_op | source)
XLA Modules:
  0.0 121.4 jit_solution(7972314391291890784)
XLA Ops:
  0.0 120.6 %shard_map.73 = bf16[128,2048]{1,0:T(8,128)(2,1)S(1)} custom-call(bf16[128,2048]{1,0:T(8,128)(2,1)} %tok_h.1, f32[4,2048]{1,0:T(4,128)} %gains_h.1, f32[1,256]{1,0:T(1,128)} %bitcast.1, bf16[512,256]{1,0:T(8,128)(2,1)} %mi_h.1, bf16[256,512]{1,0:T(8,128)(2,1)} %mo_h.1, bf16[512,2048]{1,0:T(8,128)(2,1)} %up_h.1, bf16[2048,512]{1,0:T(8,128)(2,1)} %dn_h.1), custom_call_target="tpu_custom_call" | custom-call | tf_op jit(solution)/shard_map/pallas_call | solution.py:776
  120.6 0.8 copy.9
